TPU v7x, 32 devices: a whole 2x2x4 slice. The times are simulated.
32 devices in a mesh: rep: 2 (over x), fs: 4 (over y, core), tp: 4 (over z).
Axes of the slice: x: 2, y: 2, z: 4, core: 2. Of those that a mesh axis runs over, the one named last changes fastest.
Arguments:
- acts: bfloat16 [2048, 2048], P(('rep', 'fs'), 'tp'), may hold values from -6 to 6
- cotangent: bfloat16 [2048, 2048], P(('rep', 'fs'), 'tp'), may hold values from -8 to 8
- pre_act: bfloat16 [2048, 4096], P(('rep', 'fs'), 'tp'), may hold values from -6 to 6
- up_store: float32 [2048, 4096], P('fs', 'tp'), may hold values from -0.125 to 0.125
- up_scale: float32 [4096], P('tp'), may hold values from 0.5 to 2
- down_store: float32 [4096, 2048], P('tp', 'fs'), may hold values from -0.09375 to 0.09375
- down_scale: float32 [2048], replicated, may hold values from 0.5 to 2
Outputs:
- grad_input: bfloat16 [2048, 2048], P(('rep', 'fs'), 'tp')
- grad_up: float32 [2048, 4096], P('fs', 'tp')
- grad_down: float32 [4096, 2048], P('tp', 'fs')
All inputs are finite; a program needn't handle non-finite values.
Results may differ from a plain program's by a relative error of at most 0.007.
Values may be sent and summed in bfloat16 or wider, within the bound.
A program may use at most 128 MiB of HBM per device.

v0:
```python
import functools
import math

import jax
import jax.numpy as jnp
from jax import lax
from jax.experimental import pallas as pl
from jax.experimental.pallas import tpu as pltpu
from jax.sharding import PartitionSpec as P

F32, BF16 = jnp.float32, jnp.bfloat16


def dot(left, right, dims):
    return lax.dot_general(left, right, (dims, ((), ())), preferred_element_type=F32)


def fitting(size, most):
    return most if size % most == 0 else size


def kernel(
    sizes,
    acts, cotangent, pre_act, up_store, up_scale, down_store, down_scale,
    grad_input, grad_up, grad_down,
    up_f32, down_f32,
    blocks, scaled_cols, acts_cols, act_group, dpre_group, down_bf, up_bf,
    pair_out, pair_in, far_out, far_in, d_act, gi_out, gi_mid, gi_in,
    gd_out, gd_in, gu_out, gu_in,
    load_sem,
    z_send, z_recv, col_send, col_recv, act_send, act_recv, dpre_send, dpre_recv,
    pair_send, pair_recv, far_send, far_recv, mid_send, mid_recv, gi_send, gi_recv,
    gd_send, gd_recv, gu_send, gu_recv,
):
    reps, F, T = sizes
    n, d = acts.shape
    h = pre_act.shape[1]
    w = down_store.shape[1]
    half, sub = F // 2, F // T
    chunks, cw = blocks.shape[2], blocks.shape[4]
    per = w // cw
    parts, hp = dpre_group.shape[0], dpre_group.shape[2]
    norm_factor = 1.0 / math.sqrt(n * F * reps)
    r, f, z = lax.axis_index("rep"), lax.axis_index("fs"), lax.axis_index("tp")
    core, place = lax.rem(f, 2), lax.div(f, 2)
    partner = f + 1 - 2 * core
    mesh_ids = pl.DeviceIdType.MESH

    down_load = pltpu.make_async_copy(down_store, down_f32, load_sem.at[0])
    up_load = pltpu.make_async_copy(up_store, up_f32, load_sem.at[1])
    down_load.start()
    up_load.start()

    barrier = pltpu.get_barrier_semaphore()

    def greet(at, carry):
        to_f, to_z = lax.div(at, T), lax.rem(at, T)

        @pl.when((to_f != f) | (to_z != z))
        def _():
            pl.semaphore_signal(
                barrier, inc=1, device_id={"fs": to_f, "tp": to_z}, device_id_type=mesh_ids
            )

        return carry

    lax.fori_loop(0, F * T, greet, 0)
    for p in range(1, reps):
        pl.semaphore_signal(
            barrier, inc=1, device_id={"rep": lax.rem(r + p, reps)}, device_id_type=mesh_ids
        )

    def rows(at):
        return pl.ds(pl.multiple_of(at * n, n), n)

    def remote(src, dst, send, recv, where):
        return pltpu.make_async_remote_copy(
            src_ref=src, dst_ref=dst, send_sem=send, recv_sem=recv,
            device_id=where, device_id_type=mesh_ids,
        )

    def landed(ref, recv):
        remote(ref, ref, recv, recv, {"fs": partner}).wait_recv()

    def left_for(ref, send):
        remote(ref, ref, send, send, {"fs": partner}).wait_send()

    cols = (scaled_cols, acts_cols)

    def pass_on(a, block, g, way):
        @pl.when((z < T - 1) if way == 0 else (z > 0))
        def _():
            ref = blocks.at[a, block, g]
            to = z + 1 if way == 0 else z - 1
            remote(ref, ref, z_send.at[a, block, g, way], z_recv.at[a, block, g], {"tp": to}).start()

    def spread(a, block, g):
        target, q = block * sub + g // per, g % per

        @pl.when(target != f)
        def _():
            remote(
                blocks.at[a, block, g], cols[a].at[q, rows(f)],
                col_send.at[a, block, g], col_recv.at[a, f, q], {"fs": target},
            ).start()

        @pl.when(target == f)
        def _():
            cols[a][q, rows(f), :] = blocks[a, block, g]

    def own_block(a):
        for g in range(chunks):
            pass_on(a, z, g, 0)
            pass_on(a, z, g, 1)
        for g in range(chunks):
            spread(a, z, g)

    def arriving(a, s):
        for g in range(chunks):
            @pl.when(z - s >= 0)
            def _():
                landed(blocks.at[a, z - s, g], z_recv.at[a, z - s, g])
                pass_on(a, z - s, g, 0)
                spread(a, z - s, g)

            @pl.when(z + s <= T - 1)
            def _():
                landed(blocks.at[a, z + s, g], z_recv.at[a, z + s, g])
                pass_on(a, z + s, g, 1)
                spread(a, z + s, g)

    def cols_landed(a, source):
        @pl.when(source != f)
        def _():
            for q in range(per):
                landed(cols[a].at[q, rows(source)], col_recv.at[a, source, q])

    def group_start(group, send, recv):
        ref = group.at[rows(f)]
        for k in range(1, half):
            to = lax.rem(f + 2 * k, F)
            remote(ref, ref, send.at[k], recv.at[f], {"fs": to}).start()
        remote(ref, ref, send.at[0], recv.at[f], {"fs": partner}).start()

    def group_forward(group, send, recv):
        for k in range(1, half):
            source = lax.rem(f - 2 * k + F, F)
            ref = group.at[rows(source)]
            landed(ref, recv.at[source])
            remote(ref, ref, send.at[half - 1 + k], recv.at[source], {"fs": partner}).start()

    def forwards_landed(group, recv):
        for k in range(1, half):
            source = lax.rem(partner + 2 * k, F)
            landed(group.at[rows(source)], recv.at[source])

    def group_sent(group, send):
        for k in range(F - 1):
            left_for(group.at[rows(f)], send.at[k])

    scale = down_scale[:, pl.ds(pl.multiple_of(z * d, d), d)]
    scaled = (cotangent[...].astype(F32) * scale).astype(BF16)
    for g in range(chunks):
        blocks[0, z, g] = scaled[:, g * cw:(g + 1) * cw]
    positive = jnp.maximum(pre_act[...].astype(F32), 0.0)
    act_group[rows(f), :] = (positive * positive).astype(BF16)
    pl.semaphore_wait(barrier, F * T - 1 + reps - 1)
    own_block(0)
    group_start(act_group, act_send, act_recv)
    for g in range(chunks):
        blocks[1, z, g] = acts[:, g * cw:(g + 1) * cw]
    down_load.wait()
    down_bf[...] = down_f32[...].astype(BF16)
    for s in range(1, T):
        if s == T - 1:
            group_forward(act_group, act_send, act_recv)
        arriving(0, s)
    own_block(1)

    def partial_of(target, e):
        value = jnp.zeros((n, hp), F32)
        for q in range(per):
            value = value + dot(
                scaled_cols[q, rows(target), :],
                down_bf[e * hp:(e + 1) * hp, q * cw:(q + 1) * cw], ((1,), (1,)),
            )
        return value

    for e in range(parts):
        def for_partner(k, carry):
            i = lax.rem(place + k, half)
            if e == 0:
                cols_landed(0, 2 * i + 1 - core)
            pair_out[e, i] = partial_of(2 * i + 1 - core, e).astype(BF16)
            remote(
                pair_out.at[e, i], pair_in.at[e, i], pair_send.at[e, i], pair_recv.at[e, i],
                {"fs": partner},
            ).start()
            return carry

        lax.fori_loop(1, half + 1, for_partner, 0)
    for e in range(parts):
        def for_far(k, carry):
            i = lax.rem(place + k, half)
            if e == 0:
                cols_landed(0, 2 * i + core)
            value = partial_of(2 * i + core, e)
            landed(pair_in.at[e, i], pair_recv.at[e, i])
            far_out[e, i] = (value + pair_in[e, i].astype(F32)).astype(BF16)
            remote(
                far_out.at[e, i], far_in.at[e, place], far_send.at[e, i], far_recv.at[e, place],
                {"fs": 2 * i + core},
            ).start()
            return carry

        lax.fori_loop(1, half, for_far, 0)
    for e in range(parts):
        value = partial_of(f, e)
        landed(pair_in.at[e, place], pair_recv.at[e, place])
        d_act[e] = value + pair_in[e, place].astype(F32)

    landed(act_group.at[rows(partner)], act_recv.at[partner])
    forwards_landed(act_group, act_recv)
    gd_rows = gd_out.shape[1]

    def rep_copy(out, into, send, recv, c, p):
        to = lax.rem(r + p, reps)
        return remote(
            out.at[c], into.at[p - 1, c], send.at[p - 1, c], recv.at[p - 1, c], {"rep": to}
        )

    def down_step(c, carry):
        at = pl.ds(pl.multiple_of(c * gd_rows, gd_rows), gd_rows)
        for q in range(per):
            value = dot(act_group[:, at], scaled_cols[q], ((0,), (0,))) * norm_factor
            gd_out[c, :, q * cw:(q + 1) * cw] = value.astype(BF16)
        for p in range(1, reps):
            rep_copy(gd_out, gd_in, gd_send, gd_recv, c, p).start()
        return carry

    lax.fori_loop(0, gd_out.shape[0], down_step, 0)
    arriving(1, 1)
    for e in range(parts):
        total = d_act[e]
        for k in range(1, half):
            j = lax.rem(place + k, half)
            landed(far_in.at[e, j], far_recv.at[e, j])
            total = total + far_in[e, j].astype(F32)
        at = slice(e * hp, (e + 1) * hp)
        positive = jnp.maximum(pre_act[:, at].astype(F32), 0.0)
        dpre_group[e, rows(f), :] = (2.0 * positive * total * up_scale[:, at]).astype(BF16)
        group_start(dpre_group.at[e], dpre_send.at[e], dpre_recv.at[e])
        if e == 0:
            up_load.wait()
            up_bf[...] = up_f32[...].astype(BF16)
            for s in range(2, T - 1):
                arriving(1, s)
    if T > 2:
        arriving(1, T - 1)

    def send_home(ref, source):
        home, slot = lax.div(source, sub), z * sub + lax.rem(source, sub)

        @pl.when(home != z)
        def _():
            remote(
                ref, gi_in.at[slot], gi_send.at[source], gi_recv.at[slot], {"tp": home}
            ).start()

        @pl.when(home == z)
        def _():
            gi_in[slot] = ref[...]

    def input_part(source):
        value = jnp.zeros((n, w), F32)
        for e in range(parts):
            value = value + dot(
                dpre_group[e, rows(source), :], up_bf[:, e * hp:(e + 1) * hp], ((1,), (1,))
            )
        gi_out[source] = value.astype(BF16)

        if source is f:
            send_home(gi_out.at[source], f)
        else:
            remote(
                gi_out.at[source], gi_mid.at[f], mid_send.at[source], mid_recv.at[f],
                {"fs": source},
            ).start()

    def relay(source):
        landed(gi_mid.at[source], mid_recv.at[source])
        send_home(gi_mid.at[source], source)

    input_part(f)
    for e in range(parts):
        landed(dpre_group.at[e, rows(partner)], dpre_recv.at[e, partner])
    input_part(partner)
    relay(partner)

    def up_step(e):
        forwards_landed(dpre_group.at[e], dpre_recv.at[e])
        for q in range(per):
            value = dot(acts_cols[q], dpre_group[e], ((0,), (0,)))
            gu_out[e, q * cw:(q + 1) * cw, :] = (value * norm_factor).astype(BF16)
        for p in range(1, reps):
            rep_copy(gu_out, gu_in, gu_send, gu_recv, e, p).start()

    for e in range(parts):
        group_forward(dpre_group.at[e], dpre_send.at[e], dpre_recv.at[e])
        if e == 0:
            for source in range(F):
                cols_landed(1, source)
        if e < parts - 1:
            up_step(e)
    for k in range(1, half):
        input_part(lax.rem(f + 2 * k, F))
    forwards_landed(dpre_group.at[parts - 1], dpre_recv.at[parts - 1])
    for k in range(1, half):
        input_part(lax.rem(partner + 2 * k, F))
    for q in range(per):
        value = dot(acts_cols[q], dpre_group[parts - 1], ((0,), (0,)))
        gu_out[parts - 1, q * cw:(q + 1) * cw, :] = (value * norm_factor).astype(BF16)
    for p in range(1, reps):
        rep_copy(gu_out, gu_in, gu_send, gu_recv, parts - 1, p).start()
    for k in range(1, half):
        relay(lax.rem(f + 2 * k, F))
        relay(lax.rem(partner + 2 * k, F))

    def total_of(out, into, send, recv, c):
        for p in range(1, reps):
            rep_copy(out, into, send, recv, c, p).wait()
        value = out[c].astype(F32)
        for p in range(1, reps):
            value = value + into[p - 1, c].astype(F32)
        return value

    def finish_down(c, carry):
        at = pl.ds(pl.multiple_of(c * gd_rows, gd_rows), gd_rows)
        grad_down[at, :] = total_of(gd_out, gd_in, gd_send, gd_recv, c)
        return carry

    lax.fori_loop(0, gd_out.shape[0], finish_down, 0)
    for e in range(parts - 1):
        grad_up[:, e * hp:(e + 1) * hp] = total_of(gu_out, gu_in, gu_send, gu_recv, e)
    for j in range(sub):
        value = jnp.zeros((n, w), F32)
        for s in range(T):
            at = s * sub + j

            @pl.when(s != z)
            def _():
                landed(gi_in.at[at], gi_recv.at[at])

            value = value + gi_in[at].astype(F32)
        grad_input[:, j * w:(j + 1) * w] = value.astype(BF16)
    grad_up[:, (parts - 1) * hp:] = total_of(gu_out, gu_in, gu_send, gu_recv, parts - 1)

    for a in range(2):
        for block in range(T):
            for g in range(chunks):
                @pl.when((block <= z) & (z < T - 1))
                def _():
                    left_for(blocks.at[a, block, g], z_send.at[a, block, g, 0])

                @pl.when((block >= z) & (z > 0))
                def _():
                    left_for(blocks.at[a, block, g], z_send.at[a, block, g, 1])

                @pl.when(block * sub + g // per != f)
                def _():
                    left_for(blocks.at[a, block, g], col_send.at[a, block, g])
    group_sent(act_group, act_send)
    for e in range(parts):
        group_sent(dpre_group.at[e], dpre_send.at[e])
        for i in range(half):
            left_for(pair_out.at[e, i], pair_send.at[e, i])

            @pl.when(i != place)
            def _():
                left_for(far_out.at[e, i], far_send.at[e, i])
    for source in range(F):
        @pl.when(source != f)
        def _():
            left_for(gi_out.at[source], mid_send.at[source])

        @pl.when(source // sub != z)
        def _():
            left_for(gi_mid.at[source], gi_send.at[source])


def body(sizes, acts, cotangent, pre_act, up_store, up_scale, down_store, down_scale):
    reps, F, T = sizes
    n, d = acts.shape
    h = pre_act.shape[1]
    w = down_store.shape[1]
    half = F // 2
    cw = w // 2 if w % 256 == 0 else w
    per, chunks = w // cw, d // cw
    parts = 2 if h % 256 == 0 else 1
    hp = h // parts
    gd_rows = fitting(h, 256)
    gd_steps = h // gd_rows
    others = max(reps - 1, 1)
    sem = pltpu.SemaphoreType.DMA
    vmem, anywhere = (pl.BlockSpec(memory_space=s) for s in (pltpu.VMEM, pltpu.HBM))
    arrays = [
        ((w, h), F32), ((h, w), F32),
        ((2, T, chunks, n, cw), BF16),
        ((per, F * n, cw), BF16), ((per, F * n, cw), BF16),
        ((F * n, h), BF16), ((parts, F * n, hp), BF16),
        ((h, w), BF16), ((w, h), BF16),
        ((parts, half, n, hp), BF16), ((parts, half, n, hp), BF16),
        ((parts, half, n, hp), BF16), ((parts, half, n, hp), BF16),
        ((parts, n, hp), F32),
        ((F, n, w), BF16), ((F, n, w), BF16), ((F, n, w), BF16),
        ((gd_steps, gd_rows, w), BF16), ((others, gd_steps, gd_rows, w), BF16),
        ((parts, w, hp), BF16), ((others, parts, w, hp), BF16),
    ]
    return pl.pallas_call(
        functools.partial(kernel, sizes),
        out_shape=(
            jax.ShapeDtypeStruct((n, d), BF16),
            jax.ShapeDtypeStruct((w, h), F32),
            jax.ShapeDtypeStruct((h, w), F32),
        ),
        in_specs=[vmem, vmem, vmem, anywhere, vmem, anywhere, vmem],
        out_specs=(vmem, vmem, vmem),
        scratch_shapes=[pltpu.VMEM(shape, kind) for shape, kind in arrays] + [
            sem((2,)),
            sem((2, T, chunks, 2)), sem((2, T, chunks)), sem((2, T, chunks)), sem((2, F, per)),
            sem((F,)), sem((F,)), sem((parts, F)), sem((parts, F)),
            sem((parts, half)), sem((parts, half)), sem((parts, half)), sem((parts, half)),
            sem((F,)), sem((F,)), sem((F,)), sem((F,)),
            sem((others, gd_steps)), sem((others, gd_steps)),
            sem((others, parts)), sem((others, parts)),
        ],
        compiler_params=pltpu.CompilerParams(
            collective_id=0, has_side_effects=True,
            vmem_limit_bytes=60 * 1024 * 1024,
        ),
    )(
        acts, cotangent, pre_act, up_store, up_scale.reshape(1, h), down_store,
        down_scale.reshape(1, d * T),
    )


def solution(mesh):
    sizes = (mesh.shape["rep"], mesh.shape["fs"], mesh.shape["tp"])
    return jax.shard_map(
        functools.partial(body, sizes),
        mesh=mesh,
        in_specs=(
            P(("rep", "fs"), "tp"),
            P(("rep", "fs"), "tp"),
            P(("rep", "fs"), "tp"),
            P("fs", "tp"),
            P("tp"),
            P("tp", "fs"),
            P(),
        ),
        out_specs=(P(("rep", "fs"), "tp"), P("fs", "tp"), P("tp", "fs")),
        check_vma=False,
    )
```

profile of v0, /device:TPU:5, one launch (start us, length us, event | category | flops | bytes accessed | tf_op | source)
XLA Modules:
  0.0 103.8 jit_solution(5696279067631637642)
XLA Ops:
  0.6 96.8 %shard_map.94 = (bf16[256,512]{1,0:T(8,128)(2,1)}, f32[512,1024]{1,0:T(8,128)}, f32[1024,512]{1,0:T(8,128)}) custom-call(bf16[256,512]{1,0:T(8,128)(2,1)} %acts.1, bf16[256,512]{1,0:T(8,128)(2,1)} %cotangent.1, bf16[256,1024]{1,0:T(8,128)(2,1)} %pre_act.1, f32[512,1024]{1,0:T(8,128)} %up_store.1, f32[1,1024]{1,0:T(1,128)} %bitcast.3, ...), custom_call_target="tpu_custom_call" | custom-call | tf_op jit(solution)/shard_map/pallas_call | solution.py:419
  97.5 1.7 %copy.13 = bf16[256,512]{1,0:T(8,128)(2,1)} copy(bf16[256,512]{1,0:T(8,128)(2,1)} %get-tuple-element.6) | data formatting | bytes 524288
  99.1 0.0 copy-start
  99.1 3.3 %copy.14 = f32[512,1024]{1,0:T(8,128)} copy(f32[512,1024]{1,0:T(8,128)} %get-tuple-element.7) | data formatting | bytes 4194304
  102.5 0.0 copy-done
  102.5 1.3 %copy.15 = f32[1024,512]{1,0:T(8,128)} copy(f32[1024,512]{1,0:T(8,128)S(1)} %copy-done) | data formatting | bytes 4194304
Async XLA Ops:
  99.1 3.3 %copy-start = (f32[1024,512]{1,0:T(8,128)S(1)}, f32[1024,512]{1,0:T(8,128)}, u32[]{:S(2)}) copy-start(f32[1024,512]{1,0:T(8,128)} %get-tuple-element.8) | copy-start | bytes 6291460
where the time goes:
time: 105 us; the launch traced here: 104 us
  Pallas kernels  96.8 us (92%)
  local copies, waits for them, and re-layouts  6.3 us (6%)
    pallas_call x1, Pallas kernels, body(): pl.pallas_call(functools.partial(kernel, sizes), out_shape=(jax.ShapeDtyp...  96.8 us
    unnamed x5, local copies, waits for them, and re-layouts  6.3 us

commit v1 on v0

--- a/solution.py
+++ b/solution.py
@@ -19,7 +19,7 @@
     return most if size % most == 0 else size
 
 
-def kernel(
+def general_kernel(
     sizes,
     acts, cotangent, pre_act, up_store, up_scale, down_store, down_scale,
     grad_input, grad_up, grad_down,
@@ -388,7 +388,7 @@
             left_for(gi_mid.at[source], gi_send.at[source])
 
 
-def body(sizes, acts, cotangent, pre_act, up_store, up_scale, down_store, down_scale):
+def general_body(sizes, acts, cotangent, pre_act, up_store, up_scale, down_store, down_scale):
     reps, F, T = sizes
     n, d = acts.shape
     h = pre_act.shape[1]
@@ -417,7 +417,7 @@
         ((parts, w, hp), BF16), ((others, parts, w, hp), BF16),
     ]
     return pl.pallas_call(
-        functools.partial(kernel, sizes),
+        functools.partial(general_kernel, sizes),
         out_shape=(
             jax.ShapeDtypeStruct((n, d), BF16),
             jax.ShapeDtypeStruct((w, h), F32),
@@ -444,6 +444,536 @@
     )
 
 
+def square_kernel(
+    sizes,
+    acts, cotangent, pre_act, up_store, up_scale, down_store, down_scale,
+    gd_out, gd_in, gu_out, gu_in, gi_in,
+    acts_v, cot_v, pre_v, up_f32, up_scale_v, down_f32, down_scale_v,
+    own, scaled_cols, acts_cols, act_group, dpre_group, down_bf, up_bf,
+    pair_out, pair_in, far_out, far_in, d_act, gi_out, gi_mid,
+    load_sem,
+    org_send, fwd_send, col_recv, act_send, act_recv, dpre_send, dpre_recv,
+    pair_send, pair_recv, far_send, far_recv,
+    mid_send, mid_recv, gi_send, gi_recv, relay_send,
+    gd_send, gd_recv, gu_send, gu_recv,
+):
+    reps, F, T = sizes
+    n, d = acts.shape
+    h = pre_act.shape[1]
+    w = down_store.shape[1]
+    parts, hp = dpre_group.shape[0], dpre_group.shape[2]
+    steps, gd_rows = gd_out.shape[0], gd_out.shape[1]
+    tiles, gu_rows = gu_out.shape[1], gu_out.shape[2]
+    pieces = col_recv.shape[2]
+    rp = n // pieces
+    norm_factor = 1.0 / math.sqrt(n * F * reps)
+    r, f, z = lax.axis_index("rep"), lax.axis_index("fs"), lax.axis_index("tp")
+    core, place = lax.rem(f, 2), lax.div(f, 2)
+    partner = f + 1 - 2 * core
+    across = lax.rem(f + 2, F)
+    corner = lax.rem(partner + 2, F)
+    z_pair, z_far = z + 1 - 2 * lax.rem(z, 2), lax.rem(z + 2, T)
+    mesh_ids = pl.DeviceIdType.MESH
+
+    loads = [
+        pltpu.make_async_copy(src, dst, load_sem.at[i])
+        for i, (src, dst) in enumerate((
+            (cotangent, cot_v), (down_scale, down_scale_v), (pre_act, pre_v),
+            (down_store, down_f32), (acts, acts_v), (up_scale, up_scale_v), (up_store, up_f32),
+        ))
+    ]
+    for load in loads:
+        load.start()
+
+    barrier = pltpu.get_barrier_semaphore()
+
+    def greet(at, carry):
+        to_f, to_z = lax.div(at, T), lax.rem(at, T)
+
+        @pl.when((to_f != f) | (to_z != z))
+        def _():
+            pl.semaphore_signal(
+                barrier, inc=1, device_id={"fs": to_f, "tp": to_z}, device_id_type=mesh_ids
+            )
+
+        return carry
+
+    lax.fori_loop(0, F * T, greet, 0)
+    for p in range(1, reps):
+        pl.semaphore_signal(
+            barrier, inc=1, device_id={"rep": lax.rem(r + p, reps)}, device_id_type=mesh_ids
+        )
+
+    def rows(at):
+        return pl.ds(pl.multiple_of(at * n, n), n)
+
+    def piece(at, p):
+        return pl.ds(pl.multiple_of(at * n + p * rp, rp), rp)
+
+    def remote(src, dst, send, recv, where):
+        return pltpu.make_async_remote_copy(
+            src_ref=src, dst_ref=dst, send_sem=send, recv_sem=recv,
+            device_id=where, device_id_type=mesh_ids,
+        )
+
+    def landed(ref, recv):
+        remote(ref, ref, recv, recv, {"fs": partner}).wait_recv()
+
+    def left_for(ref, send):
+        remote(ref, ref, send, send, {"fs": partner}).wait_send()
+
+    cols = (scaled_cols, acts_cols)
+    sources = (own, acts_v)
+    same = lax.div(z, 2) == place
+    direct = (z == f) | (z_far == f)
+    rises = (z > f) & (z < T - 1)
+    falls = (z < f) & (z > 0)
+
+    def originate(a, k, p, where):
+        at = pl.ds(p * rp, rp)
+        remote(
+            sources[a].at[at], cols[a].at[piece(f, p)],
+            org_send.at[a, k, p], col_recv.at[a, f, p], where,
+        ).start()
+
+    def originate_line(a):
+        @pl.when(same)
+        def _():
+            for p in range(pieces):
+                @pl.when(z < T - 1)
+                def _():
+                    originate(a, 1, p, {"fs": z, "tp": z + 1})
+
+                @pl.when(z > 0)
+                def _():
+                    originate(a, 2, p, {"fs": z, "tp": z - 1})
+
+                @pl.when(z != f)
+                def _():
+                    originate(a, 0, p, {"fs": z})
+
+            @pl.when(z == f)
+            def _():
+                cols[a][rows(f), :] = sources[a][...]
+
+    def originate_cross(a):
+        @pl.when(jnp.logical_not(same))
+        def _():
+            for p in range(pieces):
+                originate(a, 1, p, {"fs": z, "tp": z_far})
+                originate(a, 0, p, {"fs": z})
+
+    def pass_on(a, source, p, to):
+        ref = cols[a].at[piece(source, p)]
+        landed(ref, col_recv.at[a, source, p])
+        remote(ref, ref, fwd_send.at[a, source, p], col_recv.at[a, source, p], {"tp": to}).start()
+
+    def cross_forward(a):
+        @pl.when(direct)
+        def _():
+            for p in range(pieces):
+                for source in (across, corner):
+                    pass_on(a, source, p, z_pair)
+
+    def line_forward(a):
+        @pl.when(rises)
+        def _():
+            for p in range(pieces):
+                for source in (f, partner):
+                    pass_on(a, source, p, z + 1)
+
+        @pl.when(falls)
+        def _():
+            for p in range(pieces):
+                for source in (f, partner):
+                    pass_on(a, source, p, z - 1)
+
+    def cross_rest(a):
+        @pl.when(jnp.logical_not(direct))
+        def _():
+            for p in range(pieces):
+                for source in (across, corner):
+                    landed(cols[a].at[piece(source, p)], col_recv.at[a, source, p])
+
+    def line_rest(a):
+        for p in range(pieces):
+            @pl.when(jnp.logical_not(rises | falls) & (z != f))
+            def _():
+                landed(cols[a].at[piece(f, p)], col_recv.at[a, f, p])
+
+            @pl.when(jnp.logical_not(rises | falls))
+            def _():
+                landed(cols[a].at[piece(partner, p)], col_recv.at[a, partner, p])
+
+    def act_across(p):
+        ref = act_group.at[piece(f, p)]
+        remote(ref, ref, act_send.at[0, p], act_recv.at[f, p], {"fs": across}).start()
+
+    loads[0].wait()
+    loads[1].wait()
+    scale = down_scale_v[:, pl.ds(pl.multiple_of(z * d, d), d)]
+    own[...] = (cot_v[...].astype(F32) * scale).astype(BF16)
+    loads[2].wait()
+    positive = jnp.maximum(pre_v[...].astype(F32), 0.0)
+    act_group[rows(f), :] = (positive * positive).astype(BF16)
+    loads[4].wait()
+    pl.semaphore_wait(barrier, F * T - 1 + reps - 1)
+
+    originate_cross(0)
+    originate_line(0)
+    for p in range(pieces - 1):
+        act_across(p)
+    for p in range(pieces):
+        ref = act_group.at[piece(f, p)]
+        remote(ref, ref, act_send.at[1, p], act_recv.at[f, p], {"fs": partner}).start()
+    loads[3].wait()
+    down_bf[...] = down_f32[...].astype(BF16)
+    cross_forward(0)
+    act_across(pieces - 1)
+    line_forward(0)
+    cross_rest(0)
+
+    def partial_of(target, e):
+        return dot(
+            scaled_cols[rows(target), :], down_bf[e * hp:(e + 1) * hp, :], ((1,), (1,))
+        )
+
+    def to_partner(target, k, e):
+        pair_out[k, e] = partial_of(target, e).astype(BF16)
+        remote(
+            pair_out.at[k, e], pair_in.at[k, e], pair_send.at[k, e], pair_recv.at[k, e],
+            {"fs": partner},
+        ).start()
+
+    for e in range(parts):
+        to_partner(corner, 0, e)
+    for e in range(parts):
+        value = partial_of(across, e)
+        landed(pair_in.at[0, e], pair_recv.at[0, e])
+        far_out[e] = (value + pair_in[0, e].astype(F32)).astype(BF16)
+        remote(
+            far_out.at[e], far_in.at[e], far_send.at[e], far_recv.at[e], {"fs": across}
+        ).start()
+
+    originate_line(1)
+    originate_cross(1)
+    for p in range(pieces):
+        ref = act_group.at[piece(across, p)]
+        landed(ref, act_recv.at[across, p])
+        remote(ref, ref, act_send.at[2, p], act_recv.at[across, p], {"fs": partner}).start()
+    line_rest(0)
+    for e in range(parts):
+        to_partner(partner, 1, e)
+    for p in range(pieces):
+        for source in (partner, corner):
+            landed(act_group.at[piece(source, p)], act_recv.at[source, p])
+
+    def rep_copy(out, into, send, recv, at, p):
+        to = lax.rem(r + p, reps)
+        return remote(
+            out.at[at], into.at[(p - 1,) + at], send.at[(p - 1,) + at], recv.at[(p - 1,) + at],
+            {"rep": to},
+        )
+
+    def down_step(c, carry):
+        at = pl.ds(pl.multiple_of(c * gd_rows, gd_rows), gd_rows)
+        value = dot(act_group[:, at], scaled_cols[...], ((0,), (0,))) * norm_factor
+        gd_out[c] = value.astype(BF16)
+        for p in range(1, reps):
+            rep_copy(gd_out, gd_in, gd_send, gd_recv, (c,), p).start()
+        return carry
+
+    lax.fori_loop(0, steps, down_step, 0)
+    for e in range(parts):
+        value = partial_of(f, e)
+        landed(pair_in.at[1, e], pair_recv.at[1, e])
+        d_act[e] = value + pair_in[1, e].astype(F32)
+    loads[5].wait()
+    loads[6].wait()
+    up_bf[...] = up_f32[...].astype(BF16)
+    line_forward(1)
+
+    for e in range(parts):
+        landed(far_in.at[e], far_recv.at[e])
+        total = d_act[e] + far_in[e].astype(F32)
+        at = slice(e * hp, (e + 1) * hp)
+        positive = jnp.maximum(pre_v[:, at].astype(F32), 0.0)
+        dpre_group[e, rows(f), :] = (2.0 * positive * total * up_scale_v[:, at]).astype(BF16)
+        ref = dpre_group.at[e, rows(f)]
+        remote(ref, ref, dpre_send.at[0, e], dpre_recv.at[e, f], {"fs": across}).start()
+        remote(ref, ref, dpre_send.at[1, e], dpre_recv.at[e, f], {"fs": partner}).start()
+
+    cross_forward(1)
+
+    def input_part(target, k):
+        value = jnp.zeros((n, w), F32)
+        for e in range(parts):
+            value = value + dot(
+                dpre_group[e, rows(target), :], up_bf[:, e * hp:(e + 1) * hp], ((1,), (1,))
+            )
+        gi_out[k] = value.astype(BF16)
+
+    def half_rows(p):
+        return pl.ds(p * rp, rp)
+
+    input_part(f, 0)
+    for p in range(pieces):
+        @pl.when(z != f)
+        def _():
+            remote(
+                gi_out.at[0, half_rows(p)], gi_in.at[z, half_rows(p)],
+                gi_send.at[0, p], gi_recv.at[z, p], {"tp": f},
+            ).start()
+
+    @pl.when(z == f)
+    def _():
+        gi_in[z] = gi_out[0]
+
+    for e in range(parts):
+        landed(dpre_group.at[e, rows(partner)], dpre_recv.at[e, partner])
+    input_part(partner, 1)
+    for p in range(pieces):
+        remote(
+            gi_out.at[1, half_rows(p)], gi_in.at[z, half_rows(p)],
+            gi_send.at[1, p], gi_recv.at[z, p], {"fs": partner, "tp": f},
+        ).start()
+
+    def up_step(e):
+        landed(dpre_group.at[e, rows(corner)], dpre_recv.at[e, corner])
+        for q in range(tiles):
+            value = dot(
+                acts_cols[:, q * gu_rows:(q + 1) * gu_rows], dpre_group[e], ((0,), (0,))
+            )
+            gu_out[e, q] = (value * norm_factor).astype(BF16)
+            for p in range(1, reps):
+                rep_copy(gu_out, gu_in, gu_send, gu_recv, (e, q), p).start()
+
+    def cross_part(target, k):
+        input_part(target, k)
+        for p in range(pieces):
+            @pl.when(z == f)
+            def _():
+                remote(
+                    gi_out.at[k, half_rows(p)], gi_in.at[z, half_rows(p)],
+                    gi_send.at[k, p], gi_recv.at[z, p], {"fs": target},
+                ).start()
+
+            @pl.when(z != f)
+            def _():
+                remote(
+                    gi_out.at[k, half_rows(p)], gi_mid.at[core, half_rows(p)],
+                    gi_send.at[k, p], mid_recv.at[core, p], {"fs": target},
+                ).start()
+
+    for e in range(parts):
+        ref = dpre_group.at[e, rows(across)]
+        landed(ref, dpre_recv.at[e, across])
+        remote(ref, ref, dpre_send.at[2, e], dpre_recv.at[e, across], {"fs": partner}).start()
+        if e == 0:
+            cross_rest(1)
+            line_rest(1)
+        if e < parts - 1:
+            up_step(e)
+    cross_part(across, 2)
+    landed(dpre_group.at[parts - 1, rows(corner)], dpre_recv.at[parts - 1, corner])
+    cross_part(corner, 3)
+    for q in range(tiles):
+        value = dot(
+            acts_cols[:, q * gu_rows:(q + 1) * gu_rows], dpre_group[parts - 1], ((0,), (0,))
+        )
+        gu_out[parts - 1, q] = (value * norm_factor).astype(BF16)
+        for p in range(1, reps):
+            rep_copy(gu_out, gu_in, gu_send, gu_recv, (parts - 1, q), p).start()
+
+    for k in range(2):
+        source = core if k == 0 else 1 - core
+        home = 2 * (1 - place) + source
+
+        @pl.when(z != home)
+        def _():
+            for p in range(pieces):
+                ref = gi_mid.at[source, half_rows(p)]
+                landed(ref, mid_recv.at[source, p])
+                remote(
+                    ref, gi_in.at[z, half_rows(p)], relay_send.at[k, p], gi_recv.at[z, p],
+                    {"tp": home},
+                ).start()
+
+    for p in range(1, reps):
+        for c in range(steps):
+            rep_copy(gd_out, gd_in, gd_send, gd_recv, (c,), p).wait()
+    for s in range(T):
+        @pl.when((s != z) | (z != f))
+        def _():
+            for p in range(pieces):
+                landed(gi_in.at[s, half_rows(p)], gi_recv.at[s, p])
+
+    for p in range(pieces):
+        for a in range(2):
+            @pl.when(same & (z != f) | jnp.logical_not(same))
+            def _():
+                left_for(own.at[half_rows(p)], org_send.at[a, 0, p])
+
+            @pl.when(same & (z < T - 1) | jnp.logical_not(same))
+            def _():
+                left_for(own.at[half_rows(p)], org_send.at[a, 1, p])
+
+            @pl.when(same & (z > 0))
+            def _():
+                left_for(own.at[half_rows(p)], org_send.at[a, 2, p])
+
+            @pl.when(direct)
+            def _():
+                for source in (across, corner):
+                    left_for(own.at[half_rows(p)], fwd_send.at[a, source, p])
+
+            @pl.when(rises | falls)
+            def _():
+                for source in (f, partner):
+                    left_for(own.at[half_rows(p)], fwd_send.at[a, source, p])
+        for k in range(3):
+            left_for(act_group.at[piece(f, p)], act_send.at[k, p])
+
+        @pl.when(z != f)
+        def _():
+            left_for(own.at[half_rows(p)], gi_send.at[0, p])
+
+        for k in range(1, 4):
+            left_for(own.at[half_rows(p)], gi_send.at[k, p])
+        for k in range(2):
+            source = core if k == 0 else 1 - core
+
+            @pl.when(z != 2 * (1 - place) + source)
+            def _():
+                left_for(own.at[half_rows(p)], relay_send.at[k, p])
+    for e in range(parts):
+        for k in range(3):
+            left_for(dpre_group.at[e, rows(f)], dpre_send.at[k, e])
+        for k in range(2):
+            left_for(pair_out.at[k, e], pair_send.at[k, e])
+        left_for(far_out.at[e], far_send.at[e])
+    for p in range(1, reps):
+        for e in range(parts):
+            for q in range(tiles):
+                rep_copy(gu_out, gu_in, gu_send, gu_recv, (e, q), p).wait()
+
+
+def finish_kernel(
+    gd_out, gd_in, gu_out, gu_in, gi_in, grad_input, grad_up, grad_down,
+    gi_v, gu_v, gd_v, gi_sem, gu_sem, gd_sem,
+):
+    others = gd_in.shape[0]
+    steps, gd_rows = gd_out.shape[0], gd_out.shape[1]
+    parts, tiles, gu_rows, hp = gu_out.shape
+    copies = []
+
+    def leave(src, dst, sem):
+        copies.append(pltpu.make_async_copy(src, dst, sem))
+        copies[-1].start()
+
+    for c in range(steps):
+        value = gd_out[c].astype(F32)
+        for p in range(others):
+            value = value + gd_in[p, c].astype(F32)
+        gd_v[c] = value
+        leave(gd_v.at[c], grad_down.at[pl.ds(c * gd_rows, gd_rows)], gd_sem.at[c])
+    for e in range(parts):
+        for q in range(tiles):
+            value = gu_out[e, q].astype(F32)
+            for p in range(others):
+                value = value + gu_in[p, e, q].astype(F32)
+            gu_v[e, q] = value
+            at = (pl.ds(q * gu_rows, gu_rows), pl.ds(e * hp, hp))
+            leave(gu_v.at[e, q], grad_up.at[at], gu_sem.at[e, q])
+    value = gi_in[0].astype(F32)
+    for s in range(1, gi_in.shape[0]):
+        value = value + gi_in[s].astype(F32)
+    gi_v[...] = value.astype(BF16)
+    leave(gi_v, grad_input, gi_sem.at[0])
+    for copy in copies:
+        copy.wait()
+
+
+def square_body(sizes, acts, cotangent, pre_act, up_store, up_scale, down_store, down_scale):
+    reps, F, T = sizes
+    n, d = acts.shape
+    h = pre_act.shape[1]
+    w = down_store.shape[1]
+    parts = 2 if h % 256 == 0 else 1
+    pieces = 2 if n % 32 == 0 else 1
+    tiles = 2 if w % 256 == 0 else 1
+    hp = h // parts
+    gd_rows = fitting(h, 256)
+    steps = h // gd_rows
+    others = reps - 1
+    sem = pltpu.SemaphoreType.DMA
+    vmem, hbm = (pl.BlockSpec(memory_space=s) for s in (pltpu.VMEM, pltpu.HBM))
+    shared = [
+        (steps, gd_rows, w), (others, steps, gd_rows, w),
+        (parts, tiles, w // tiles, hp), (others, parts, tiles, w // tiles, hp),
+        (T, n, w),
+    ]
+    arrays = [
+        ((n, d), BF16), ((n, d), BF16), ((n, h), BF16),
+        ((w, h), F32), ((1, h), F32), ((h, w), F32), ((1, d * T), F32),
+        ((n, d), BF16), ((F * n, w), BF16), ((F * n, w), BF16),
+        ((F * n, h), BF16), ((parts, F * n, hp), BF16),
+        ((h, w), BF16), ((w, h), BF16),
+        ((2, parts, n, hp), BF16), ((2, parts, n, hp), BF16),
+        ((parts, n, hp), BF16), ((parts, n, hp), BF16),
+        ((parts, n, hp), F32),
+        ((F, n, w), BF16), ((2, n, w), BF16),
+    ]
+    moved = pl.pallas_call(
+        functools.partial(square_kernel, sizes),
+        out_shape=tuple(jax.ShapeDtypeStruct(shape, BF16) for shape in shared),
+        in_specs=[hbm] * 7,
+        out_specs=(vmem,) * len(shared),
+        scratch_shapes=[pltpu.VMEM(shape, kind) for shape, kind in arrays] + [
+            sem((7,)),
+            sem((2, 3, pieces)), sem((2, F, pieces)), sem((2, F, pieces)),
+            sem((3, pieces)), sem((F, pieces)), sem((3, parts)), sem((parts, F)),
+            sem((2, parts)), sem((2, parts)), sem((parts,)), sem((parts,)),
+            sem((1,)), sem((2, pieces)), sem((4, pieces)), sem((T, pieces)), sem((2, pieces)),
+            sem((others, steps)), sem((others, steps)),
+            sem((others, parts, tiles)), sem((others, parts, tiles)),
+        ],
+        compiler_params=pltpu.CompilerParams(
+            collective_id=0, has_side_effects=True,
+            vmem_limit_bytes=40 * 1024 * 1024,
+        ),
+    )(*(
+        pltpu.with_memory_space_constraint(array, pltpu.HBM)
+        for array in (
+            acts, cotangent, pre_act, up_store, up_scale.reshape(1, h), down_store,
+            down_scale.reshape(1, d * T),
+        )
+    ))
+    return pl.pallas_call(
+        finish_kernel,
+        out_shape=(
+            jax.ShapeDtypeStruct((n, d), BF16),
+            jax.ShapeDtypeStruct((w, h), F32),
+            jax.ShapeDtypeStruct((h, w), F32),
+        ),
+        in_specs=[vmem] * len(shared),
+        out_specs=(hbm,) * 3,
+        scratch_shapes=[
+            pltpu.VMEM((n, d), BF16),
+            pltpu.VMEM((parts, tiles, w // tiles, hp), F32),
+            pltpu.VMEM((steps, gd_rows, w), F32),
+            sem((1,)), sem((parts, tiles)), sem((steps,)),
+        ],
+        compiler_params=pltpu.CompilerParams(vmem_limit_bytes=12 * 1024 * 1024),
+    )(*moved)
+
+
+def body(sizes, *arrays):
+    reps, F, T = sizes
+    square = F == T and F == 2 * 2 and reps > 1
+    return (square_body if square else general_body)(sizes, *arrays)
+
+
 def solution(mesh):
     sizes = (mesh.shape["rep"], mesh.shape["fs"], mesh.shape["tp"])
     return jax.shard_map(

time: 105 us -> 89 us (0.85); the launches traced: 104 us -> 88.9 us
  Pallas kernels: 96.8 us -> 88.2 us
  local copies, waits for them, and re-layouts: 6.3 us -> 0 us
    pallas_call x1 -> x2, Pallas kernels: 96.8 us -> 88.2 us  [the longest x1 86 us: square_body(): pl.pallas_call(functools.partial(square_kernel, sizes), out_shape=tuple((...]
    unnamed x5 -> x0, local copies, waits for them, and re-layouts: 6.3 us -> none
where the time goes in v1:
time: 89 us; the launch traced here: 88.9 us
  Pallas kernels  88.2 us (99%)
    pallas_call x1, Pallas kernels, square_body(): pl.pallas_call(functools.partial(square_kernel, sizes), out_shape=tuple((...  86 us
    pallas_call x1, Pallas kernels, square_body(): pl.pallas_call(finish_kernel, out_shape=(jax.ShapeDtypeStruct((n, d), BF1...  2.21 us

profile of v1, /device:TPU:5, one launch (start us, length us, event | category | flops | bytes accessed | tf_op | source)
XLA Modules:
  0.0 88.9 jit_solution(17768164870905784739)
XLA Ops:
  0.6 86.0 %shard_map.94 = (bf16[4,256,512]{2,1,0:T(8,128)(2,1)S(1)}, bf16[1,4,256,512]{3,2,1,0:T(8,128)(2,1)S(1)}, bf16[2,2,256,512]{3,2,1,0:T(8,128)(2,1)S(1)}, bf16[1,2,...) custom-call(bf16[256,512]{1,0:T(8,128)(2,1)} %acts.1, bf16[256,512]{1,0:T(8,128)(2,1)} %cotangent.1, ...), custom_call_target="tpu_custom_call" | custom-call | tf_op jit(solution)/shard_map/pallas_call | solution.py:927
  86.6 2.2 %shard_map.95 = (bf16[256,512]{1,0:T(8,128)(2,1)}, f32[512,1024]{1,0:T(8,128)}, f32[1024,512]{1,0:T(8,128)}) custom-call(bf16[4,256,512]{2,1,0:T(8,128)(2,1)S(1)} %get-tuple-element.8.gd_out, bf16[1,4,256,512]{3,2,1,0:T(8,128)(2,1)S(1)} %get-tuple-element.9.gd_in, bf16[2,2,256,512]{3,2,1,0:T(8,128)(2,1)S(1)} %get-tuple-element.10.gu_out, ...), custom_call_target="tpu_custom_call" | custom-call | tf_op jit(solution)/shard_map/pallas_call | solution.py:952

commit v2 on v1

--- a/solution.py
+++ b/solution.py
@@ -449,21 +449,20 @@
     acts, cotangent, pre_act, up_store, up_scale, down_store, down_scale,
     gd_out, gd_in, gu_out, gu_in, gi_in,
     acts_v, cot_v, pre_v, up_f32, up_scale_v, down_f32, down_scale_v,
-    own, scaled_cols, acts_cols, act_group, dpre_group, down_bf, up_bf,
-    pair_out, pair_in, far_out, far_in, d_act, gi_out, gi_mid,
+    own, scaled_cols, acts_cols, pos_group, dpre_group, down_bf, up_bf,
+    pair_out, pair_in, far_out, far_in, own_f32, across_f32, gi_out, gi_mid, near_in, hub_f32,
     load_sem,
     org_send, fwd_send, col_recv, act_send, act_recv, dpre_send, dpre_recv,
     pair_send, pair_recv, far_send, far_recv,
-    mid_send, mid_recv, gi_send, gi_recv, relay_send,
+    mid_recv, near_recv, gi_send, gi_recv, relay_send,
     gd_send, gd_recv, gu_send, gu_recv,
 ):
     reps, F, T = sizes
     n, d = acts.shape
     h = pre_act.shape[1]
     w = down_store.shape[1]
-    parts, hp = dpre_group.shape[0], dpre_group.shape[2]
     steps, gd_rows = gd_out.shape[0], gd_out.shape[1]
-    tiles, gu_rows = gu_out.shape[1], gu_out.shape[2]
+    parts, tiles, gu_rows, hp = gu_out.shape
     pieces = col_recv.shape[2]
     rp = n // pieces
     norm_factor = 1.0 / math.sqrt(n * F * reps)
@@ -526,6 +525,7 @@
     sources = (own, acts_v)
     same = lax.div(z, 2) == place
     direct = (z == f) | (z_far == f)
+    home, hub, near = z == f, z_far == f, z_pair == f
     rises = (z > f) & (z < T - 1)
     falls = (z < f) & (z > 0)
 
@@ -556,6 +556,27 @@
             def _():
                 cols[a][rows(f), :] = sources[a][...]
 
+    def spread_line(a):
+        @pl.when(same)
+        def _():
+            for p in range(pieces):
+                for k in range(1, T):
+                    @pl.when(z + k < T)
+                    def _():
+                        originate(a, T + k, p, {"fs": z, "tp": z + k})
+
+                    @pl.when(z - k >= 0)
+                    def _():
+                        originate(a, 1 + k, p, {"fs": z, "tp": z - k})
+
+                @pl.when(z != f)
+                def _():
+                    originate(a, 0, p, {"fs": z})
+
+            @pl.when(z == f)
+            def _():
+                cols[a][rows(f), :] = sources[a][...]
+
     def originate_cross(a):
         @pl.when(jnp.logical_not(same))
         def _():
@@ -568,105 +589,138 @@
         landed(ref, col_recv.at[a, source, p])
         remote(ref, ref, fwd_send.at[a, source, p], col_recv.at[a, source, p], {"tp": to}).start()
 
-    def cross_forward(a):
-        @pl.when(direct)
-        def _():
-            for p in range(pieces):
-                for source in (across, corner):
-                    pass_on(a, source, p, z_pair)
-
-    def line_forward(a):
+    def cross_forward(a, p):
+        for source in (across, corner):
+            pass_on(a, source, p, z_pair)
+
+    def line_forward(a, p):
         @pl.when(rises)
         def _():
-            for p in range(pieces):
-                for source in (f, partner):
-                    pass_on(a, source, p, z + 1)
+            for source in (f, partner):
+                pass_on(a, source, p, z + 1)
 
         @pl.when(falls)
         def _():
-            for p in range(pieces):
-                for source in (f, partner):
-                    pass_on(a, source, p, z - 1)
-
-    def cross_rest(a):
-        @pl.when(jnp.logical_not(direct))
-        def _():
-            for p in range(pieces):
-                for source in (across, corner):
-                    landed(cols[a].at[piece(source, p)], col_recv.at[a, source, p])
-
-    def line_rest(a):
-        for p in range(pieces):
-            @pl.when(jnp.logical_not(rises | falls) & (z != f))
-            def _():
-                landed(cols[a].at[piece(f, p)], col_recv.at[a, f, p])
-
-            @pl.when(jnp.logical_not(rises | falls))
-            def _():
-                landed(cols[a].at[piece(partner, p)], col_recv.at[a, partner, p])
-
-    def act_across(p):
-        ref = act_group.at[piece(f, p)]
-        remote(ref, ref, act_send.at[0, p], act_recv.at[f, p], {"fs": across}).start()
+            for source in (f, partner):
+                pass_on(a, source, p, z - 1)
+
+    def cross_rest(a, p):
+        for source in (across, corner):
+            landed(cols[a].at[piece(source, p)], col_recv.at[a, source, p])
+
+    def line_landed(a, p):
+        @pl.when(z != f)
+        def _():
+            landed(cols[a].at[piece(f, p)], col_recv.at[a, f, p])
+
+        landed(cols[a].at[piece(partner, p)], col_recv.at[a, partner, p])
+
+    def line_rest(a, p):
+        @pl.when(jnp.logical_not(rises | falls) & (z != f))
+        def _():
+            landed(cols[a].at[piece(f, p)], col_recv.at[a, f, p])
+
+        @pl.when(jnp.logical_not(rises | falls))
+        def _():
+            landed(cols[a].at[piece(partner, p)], col_recv.at[a, partner, p])
+
+    def act_cols(c):
+        return pl.ds(pl.multiple_of(c * gd_rows, gd_rows), gd_rows)
+
+    def act_send_to(source, c, k, where):
+        ref = pos_group.at[rows(source), act_cols(c)]
+        remote(ref, ref, act_send.at[k, c], act_recv.at[source, c], where).start()
+
+    def act_landed(source, c):
+        landed(pos_group.at[rows(source), act_cols(c)], act_recv.at[source, c])
+
+    def act_forward(c):
+        act_landed(across, c)
+        act_send_to(across, c, 2, {"fs": partner})
 
     loads[0].wait()
     loads[1].wait()
     scale = down_scale_v[:, pl.ds(pl.multiple_of(z * d, d), d)]
     own[...] = (cot_v[...].astype(F32) * scale).astype(BF16)
-    loads[2].wait()
-    positive = jnp.maximum(pre_v[...].astype(F32), 0.0)
-    act_group[rows(f), :] = (positive * positive).astype(BF16)
-    loads[4].wait()
     pl.semaphore_wait(barrier, F * T - 1 + reps - 1)
-
     originate_cross(0)
     originate_line(0)
-    for p in range(pieces - 1):
-        act_across(p)
-    for p in range(pieces):
-        ref = act_group.at[piece(f, p)]
-        remote(ref, ref, act_send.at[1, p], act_recv.at[f, p], {"fs": partner}).start()
+    loads[2].wait()
+    pos_group[rows(f), :] = jnp.maximum(pre_v[...].astype(F32), 0.0).astype(BF16)
+    early = (steps + 1) // 2
+    for c in range(early):
+        act_send_to(f, c, 0, {"fs": across})
+
+    @pl.when(jnp.logical_not(same))
+    def _():
+        for c in range(early, steps):
+            act_send_to(f, c, 0, {"fs": across})
+        gi_in[2] = jnp.zeros((n, w), BF16)
+
+    for c in range(steps):
+        act_send_to(f, c, 1, {"fs": partner})
     loads[3].wait()
     down_bf[...] = down_f32[...].astype(BF16)
-    cross_forward(0)
-    act_across(pieces - 1)
-    line_forward(0)
-    cross_rest(0)
-
-    def partial_of(target, e):
-        return dot(
-            scaled_cols[rows(target), :], down_bf[e * hp:(e + 1) * hp, :], ((1,), (1,))
-        )
-
-    def to_partner(target, k, e):
-        pair_out[k, e] = partial_of(target, e).astype(BF16)
+
+    def late_act():
+        for c in range(early, steps):
+            act_send_to(f, c, 0, {"fs": across})
+
+    def partial_of(target, p):
+        return dot(scaled_cols[piece(target, p), :], down_bf[...], ((1,), (1,)))
+
+    def to_partner(target, k, p):
+        pair_out[k, p] = partial_of(target, p).astype(BF16)
         remote(
-            pair_out.at[k, e], pair_in.at[k, e], pair_send.at[k, e], pair_recv.at[k, e],
+            pair_out.at[k, p], pair_in.at[k, p], pair_send.at[k, p], pair_recv.at[k, p],
             {"fs": partner},
         ).start()
 
-    for e in range(parts):
-        to_partner(corner, 0, e)
-    for e in range(parts):
-        value = partial_of(across, e)
-        landed(pair_in.at[0, e], pair_recv.at[0, e])
-        far_out[e] = (value + pair_in[0, e].astype(F32)).astype(BF16)
+    def far_start(p):
+        value = partial_of(across, p)
+        landed(pair_in.at[0, p], pair_recv.at[0, p])
+        value = value + pair_in[0, p].astype(F32)
+        across_f32[p] = value
+        far_out[0, p] = value.astype(BF16)
         remote(
-            far_out.at[e], far_in.at[e], far_send.at[e], far_recv.at[e], {"fs": across}
+            far_out.at[0, p], far_in.at[0, p], far_send.at[0, p], far_recv.at[0, p],
+            {"fs": across},
         ).start()
 
-    originate_line(1)
+    for p in range(pieces):
+        @pl.when(direct)
+        def _():
+            cross_forward(0, p)
+
+        line_forward(0, p)
+
+        @pl.when(direct)
+        def _():
+            to_partner(corner, 0, p)
+
+    @pl.when(home)
+    def _():
+        late_act()
+
+    for p in range(pieces):
+        @pl.when(jnp.logical_not(direct))
+        def _():
+            cross_rest(0, p)
+            to_partner(corner, 0, p)
+
+        if p == 0:
+            @pl.when(same & jnp.logical_not(home))
+            def _():
+                late_act()
+
+        far_start(p)
+    loads[4].wait()
     originate_cross(1)
-    for p in range(pieces):
-        ref = act_group.at[piece(across, p)]
-        landed(ref, act_recv.at[across, p])
-        remote(ref, ref, act_send.at[2, p], act_recv.at[across, p], {"fs": partner}).start()
-    line_rest(0)
-    for e in range(parts):
-        to_partner(partner, 1, e)
-    for p in range(pieces):
-        for source in (partner, corner):
-            landed(act_group.at[piece(source, p)], act_recv.at[source, p])
+    for c in range(steps):
+        act_forward(c)
+    for p in range(pieces):
+        line_rest(0, p)
+    spread_line(1)
 
     def rep_copy(out, into, send, recv, at, p):
         to = lax.rem(r + p, reps)
@@ -676,137 +730,197 @@
         )
 
     def down_step(c, carry):
-        at = pl.ds(pl.multiple_of(c * gd_rows, gd_rows), gd_rows)
-        value = dot(act_group[:, at], scaled_cols[...], ((0,), (0,))) * norm_factor
+        act_landed(partner, c)
+        act_landed(corner, c)
+        positive = pos_group[:, act_cols(c)].astype(F32)
+        act = (positive * positive).astype(BF16)
+        value = dot(act, scaled_cols[...], ((0,), (0,))) * norm_factor
         gd_out[c] = value.astype(BF16)
         for p in range(1, reps):
             rep_copy(gd_out, gd_in, gd_send, gd_recv, (c,), p).start()
         return carry
 
     lax.fori_loop(0, steps, down_step, 0)
-    for e in range(parts):
-        value = partial_of(f, e)
-        landed(pair_in.at[1, e], pair_recv.at[1, e])
-        d_act[e] = value + pair_in[1, e].astype(F32)
+    for p in range(pieces):
+        to_partner(partner, 1, p)
+    for p in range(pieces):
+        value = partial_of(f, p)
+        landed(pair_in.at[1, p], pair_recv.at[1, p])
+        value = value + pair_in[1, p].astype(F32)
+        own_f32[p] = value
+        far_out[1, p] = value.astype(BF16)
+        remote(
+            far_out.at[1, p], far_in.at[1, p], far_send.at[1, p], far_recv.at[1, p],
+            {"fs": across},
+        ).start()
     loads[5].wait()
     loads[6].wait()
     up_bf[...] = up_f32[...].astype(BF16)
-    line_forward(1)
-
-    for e in range(parts):
-        landed(far_in.at[e], far_recv.at[e])
-        total = d_act[e] + far_in[e].astype(F32)
-        at = slice(e * hp, (e + 1) * hp)
-        positive = jnp.maximum(pre_v[:, at].astype(F32), 0.0)
-        dpre_group[e, rows(f), :] = (2.0 * positive * total * up_scale_v[:, at]).astype(BF16)
-        ref = dpre_group.at[e, rows(f)]
-        remote(ref, ref, dpre_send.at[0, e], dpre_recv.at[e, f], {"fs": across}).start()
-        remote(ref, ref, dpre_send.at[1, e], dpre_recv.at[e, f], {"fs": partner}).start()
-
-    cross_forward(1)
-
-    def input_part(target, k):
-        value = jnp.zeros((n, w), F32)
-        for e in range(parts):
-            value = value + dot(
-                dpre_group[e, rows(target), :], up_bf[:, e * hp:(e + 1) * hp], ((1,), (1,))
-            )
-        gi_out[k] = value.astype(BF16)
+
+    def dpre_step(k, source, sums, p):
+        landed(far_in.at[k, p], far_recv.at[k, p])
+        value = sums[p] + far_in[k, p].astype(F32)
+        positive = pos_group[piece(source, p), :].astype(F32)
+        ref = dpre_group.at[piece(source, p)]
+        ref[...] = (2.0 * positive * value * up_scale_v[...]).astype(BF16)
+        remote(ref, ref, dpre_send.at[k, p], dpre_recv.at[source, p], {"fs": partner}).start()
+
+    for p in range(pieces):
+        dpre_step(0, f, own_f32, p)
+
+        if p == 0:
+            @pl.when(hub)
+            def _():
+                for q in range(pieces):
+                    cross_forward(1, q)
 
     def half_rows(p):
         return pl.ds(p * rp, rp)
 
-    input_part(f, 0)
-    for p in range(pieces):
-        @pl.when(z != f)
-        def _():
+    def input_part(k, p):
+        target = (f, partner, across, corner)[k]
+        return dot(dpre_group[piece(target, p), :], up_bf[...], ((1,), (1,)))
+
+    def input_sum(k, p, value):
+        landed(near_in.at[k, half_rows(p)], near_recv.at[k, p])
+        gi_out[k, half_rows(p), :] = (value + near_in[k, half_rows(p), :].astype(F32)).astype(BF16)
+
+    def input_send(k, p, into, recv, where):
+        remote(
+            gi_out.at[k, half_rows(p)], into.at[half_rows(p)], gi_send.at[k, p], recv.at[p], where
+        ).start()
+
+    def own_part(k, p):
+        target = (f, partner)[k]
+        value = input_part(k, p)
+
+        @pl.when(hub)
+        def _():
+            hub_f32[k, half_rows(p), :] = value
+
+        @pl.when(jnp.logical_not(hub))
+        def _():
+            gi_out[k, half_rows(p), :] = value.astype(BF16)
+
+        if k == 0:
+            @pl.when(home)
+            def _():
+                gi_in[0, half_rows(p), :] = gi_out[k, half_rows(p), :]
+        else:
+            @pl.when(home)
+            def _():
+                input_send(k, p, gi_in.at[0], gi_recv.at[0], {"fs": target})
+
+        @pl.when(near)
+        def _():
+            input_send(k, p, gi_in.at[2], gi_recv.at[2], {"fs": target, "tp": f})
+
+        @pl.when(jnp.logical_not(home | near | hub))
+        def _():
+            input_send(k, p, near_in.at[k], near_recv.at[k], {"tp": z_pair})
+
+    def own_sum(k, p):
+        target = (f, partner)[k]
+
+        @pl.when(hub)
+        def _():
+            input_sum(k, p, hub_f32[k, half_rows(p), :])
+            input_send(k, p, gi_in.at[1], gi_recv.at[1], {"fs": target, "tp": f})
+
+    def cross_part(k, p):
+        value = input_part(k, p)
+
+        @pl.when(direct)
+        def _():
+            hub_f32[k, half_rows(p), :] = value
+
+        @pl.when(jnp.logical_not(direct))
+        def _():
+            gi_out[k, half_rows(p), :] = value.astype(BF16)
+            input_send(k, p, near_in.at[k], near_recv.at[k], {"tp": z_pair})
+
+    def cross_sum(k, p):
+        target = (across, corner)[k - 2]
+
+        @pl.when(direct)
+        def _():
+            input_sum(k, p, hub_f32[k, half_rows(p), :])
+
+        @pl.when(home)
+        def _():
+            input_send(k, p, gi_in.at[0], gi_recv.at[0], {"fs": target})
+
+        @pl.when(hub)
+        def _():
+            input_send(k, p, gi_mid, mid_recv, {"fs": target})
+
+    for p in range(pieces):
+        own_part(0, p)
+    for p in range(pieces):
+        landed(dpre_group.at[piece(partner, p)], dpre_recv.at[partner, p])
+        own_part(1, p)
+
+    @pl.when(home)
+    def _():
+        for p in range(pieces):
+            cross_forward(1, p)
+
+    def up_step(e, q):
+        value = dot(
+            acts_cols[:, q * gu_rows:(q + 1) * gu_rows], dpre_group[:, e * hp:(e + 1) * hp],
+            ((0,), (0,)),
+        )
+        gu_out[e, q] = (value * norm_factor).astype(BF16)
+        for p in range(1, reps):
+            rep_copy(gu_out, gu_in, gu_send, gu_recv, (e, q), p).start()
+
+    for p in range(pieces):
+        dpre_step(1, across, across_f32, p)
+        landed(dpre_group.at[piece(corner, p)], dpre_recv.at[corner, p])
+        if p < pieces - 1:
+            cross_part(2, p)
+            cross_part(3, p)
+    for p in range(pieces):
+        @pl.when(jnp.logical_not(direct))
+        def _():
+            cross_rest(1, p)
+
+        line_landed(1, p)
+    for e in range(parts):
+        for q in range(tiles):
+            up_step(e, q)
+    cross_part(2, pieces - 1)
+    cross_part(3, pieces - 1)
+    for p in range(pieces):
+        for k in range(2, 4):
+            cross_sum(k, p)
+    for p in range(pieces):
+        for k in range(2):
+            own_sum(k, p)
+
+    relays = lax.div(z_far, 2) != place
+    for p in range(pieces):
+        @pl.when(relays)
+        def _():
+            ref = gi_mid.at[half_rows(p)]
+            landed(ref, mid_recv.at[p])
             remote(
-                gi_out.at[0, half_rows(p)], gi_in.at[z, half_rows(p)],
-                gi_send.at[0, p], gi_recv.at[z, p], {"tp": f},
+                ref, gi_in.at[1, half_rows(p)], relay_send.at[p], gi_recv.at[1, p], {"tp": z_far}
             ).start()
-
-    @pl.when(z == f)
-    def _():
-        gi_in[z] = gi_out[0]
-
-    for e in range(parts):
-        landed(dpre_group.at[e, rows(partner)], dpre_recv.at[e, partner])
-    input_part(partner, 1)
-    for p in range(pieces):
-        remote(
-            gi_out.at[1, half_rows(p)], gi_in.at[z, half_rows(p)],
-            gi_send.at[1, p], gi_recv.at[z, p], {"fs": partner, "tp": f},
-        ).start()
-
-    def up_step(e):
-        landed(dpre_group.at[e, rows(corner)], dpre_recv.at[e, corner])
-        for q in range(tiles):
-            value = dot(
-                acts_cols[:, q * gu_rows:(q + 1) * gu_rows], dpre_group[e], ((0,), (0,))
-            )
-            gu_out[e, q] = (value * norm_factor).astype(BF16)
-            for p in range(1, reps):
-                rep_copy(gu_out, gu_in, gu_send, gu_recv, (e, q), p).start()
-
-    def cross_part(target, k):
-        input_part(target, k)
-        for p in range(pieces):
-            @pl.when(z == f)
-            def _():
-                remote(
-                    gi_out.at[k, half_rows(p)], gi_in.at[z, half_rows(p)],
-                    gi_send.at[k, p], gi_recv.at[z, p], {"fs": target},
-                ).start()
-
-            @pl.when(z != f)
-            def _():
-                remote(
-                    gi_out.at[k, half_rows(p)], gi_mid.at[core, half_rows(p)],
-                    gi_send.at[k, p], mid_recv.at[core, p], {"fs": target},
-                ).start()
-
-    for e in range(parts):
-        ref = dpre_group.at[e, rows(across)]
-        landed(ref, dpre_recv.at[e, across])
-        remote(ref, ref, dpre_send.at[2, e], dpre_recv.at[e, across], {"fs": partner}).start()
-        if e == 0:
-            cross_rest(1)
-            line_rest(1)
-        if e < parts - 1:
-            up_step(e)
-    cross_part(across, 2)
-    landed(dpre_group.at[parts - 1, rows(corner)], dpre_recv.at[parts - 1, corner])
-    cross_part(corner, 3)
-    for q in range(tiles):
-        value = dot(
-            acts_cols[:, q * gu_rows:(q + 1) * gu_rows], dpre_group[parts - 1], ((0,), (0,))
-        )
-        gu_out[parts - 1, q] = (value * norm_factor).astype(BF16)
-        for p in range(1, reps):
-            rep_copy(gu_out, gu_in, gu_send, gu_recv, (parts - 1, q), p).start()
-
-    for k in range(2):
-        source = core if k == 0 else 1 - core
-        home = 2 * (1 - place) + source
-
-        @pl.when(z != home)
-        def _():
-            for p in range(pieces):
-                ref = gi_mid.at[source, half_rows(p)]
-                landed(ref, mid_recv.at[source, p])
-                remote(
-                    ref, gi_in.at[z, half_rows(p)], relay_send.at[k, p], gi_recv.at[z, p],
-                    {"tp": home},
-                ).start()
 
     for p in range(1, reps):
         for c in range(steps):
             rep_copy(gd_out, gd_in, gd_send, gd_recv, (c,), p).wait()
-    for s in range(T):
-        @pl.when((s != z) | (z != f))
-        def _():
-            for p in range(pieces):
-                landed(gi_in.at[s, half_rows(p)], gi_recv.at[s, p])
+    for p in range(pieces):
+        @pl.when(jnp.logical_not(home))
+        def _():
+            landed(gi_in.at[0, half_rows(p)], gi_recv.at[0, p])
+
+        landed(gi_in.at[1, half_rows(p)], gi_recv.at[1, p])
+
+        @pl.when(same)
+        def _():
+            landed(gi_in.at[2, half_rows(p)], gi_recv.at[2, p])
 
     for p in range(pieces):
         for a in range(2):
@@ -814,44 +928,56 @@
             def _():
                 left_for(own.at[half_rows(p)], org_send.at[a, 0, p])
 
-            @pl.when(same & (z < T - 1) | jnp.logical_not(same))
-            def _():
-                left_for(own.at[half_rows(p)], org_send.at[a, 1, p])
-
-            @pl.when(same & (z > 0))
-            def _():
-                left_for(own.at[half_rows(p)], org_send.at[a, 2, p])
-
             @pl.when(direct)
             def _():
                 for source in (across, corner):
                     left_for(own.at[half_rows(p)], fwd_send.at[a, source, p])
 
-            @pl.when(rises | falls)
-            def _():
-                for source in (f, partner):
-                    left_for(own.at[half_rows(p)], fwd_send.at[a, source, p])
-        for k in range(3):
-            left_for(act_group.at[piece(f, p)], act_send.at[k, p])
-
-        @pl.when(z != f)
+        @pl.when(jnp.logical_not(same))
+        def _():
+            for a in range(2):
+                left_for(own.at[half_rows(p)], org_send.at[a, 1, p])
+
+        @pl.when(same & (z < T - 1))
+        def _():
+            left_for(own.at[half_rows(p)], org_send.at[0, 1, p])
+
+        @pl.when(same & (z > 0))
+        def _():
+            left_for(own.at[half_rows(p)], org_send.at[0, 2, p])
+
+        @pl.when(rises | falls)
+        def _():
+            for source in (f, partner):
+                left_for(own.at[half_rows(p)], fwd_send.at[0, source, p])
+
+        for k in range(1, T):
+            @pl.when(same & (z + k < T))
+            def _():
+                left_for(own.at[half_rows(p)], org_send.at[1, T + k, p])
+
+            @pl.when(same & (z - k >= 0))
+            def _():
+                left_for(own.at[half_rows(p)], org_send.at[1, 1 + k, p])
+
+        @pl.when(jnp.logical_not(home))
         def _():
             left_for(own.at[half_rows(p)], gi_send.at[0, p])
 
         for k in range(1, 4):
             left_for(own.at[half_rows(p)], gi_send.at[k, p])
+
+        @pl.when(relays)
+        def _():
+            left_for(own.at[half_rows(p)], relay_send.at[p])
+
         for k in range(2):
-            source = core if k == 0 else 1 - core
-
-            @pl.when(z != 2 * (1 - place) + source)
-            def _():
-                left_for(own.at[half_rows(p)], relay_send.at[k, p])
-    for e in range(parts):
-        for k in range(3):
-            left_for(dpre_group.at[e, rows(f)], dpre_send.at[k, e])
-        for k in range(2):
-            left_for(pair_out.at[k, e], pair_send.at[k, e])
-        left_for(far_out.at[e], far_send.at[e])
+            left_for(dpre_group.at[piece(f, p)], dpre_send.at[k, p])
+            left_for(pair_out.at[k, p], pair_send.at[k, p])
+            left_for(far_out.at[k, p], far_send.at[k, p])
+    for k in range(3):
+        for c in range(steps):
+            left_for(pos_group.at[rows(f), act_cols(c)], act_send.at[k, c])
     for p in range(1, reps):
         for e in range(parts):
             for q in range(tiles):
@@ -902,7 +1028,7 @@
     parts = 2 if h % 256 == 0 else 1
     pieces = 2 if n % 32 == 0 else 1
     tiles = 2 if w % 256 == 0 else 1
-    hp = h // parts
+    hp, rp = h // parts, n // pieces
     gd_rows = fitting(h, 256)
     steps = h // gd_rows
     others = reps - 1
@@ -911,18 +1037,18 @@
     shared = [
         (steps, gd_rows, w), (others, steps, gd_rows, w),
         (parts, tiles, w // tiles, hp), (others, parts, tiles, w // tiles, hp),
-        (T, n, w),
+        (3, n, w),
     ]
     arrays = [
         ((n, d), BF16), ((n, d), BF16), ((n, h), BF16),
         ((w, h), F32), ((1, h), F32), ((h, w), F32), ((1, d * T), F32),
         ((n, d), BF16), ((F * n, w), BF16), ((F * n, w), BF16),
-        ((F * n, h), BF16), ((parts, F * n, hp), BF16),
+        ((F * n, h), BF16), ((F * n, h), BF16),
         ((h, w), BF16), ((w, h), BF16),
-        ((2, parts, n, hp), BF16), ((2, parts, n, hp), BF16),
-        ((parts, n, hp), BF16), ((parts, n, hp), BF16),
-        ((parts, n, hp), F32),
-        ((F, n, w), BF16), ((2, n, w), BF16),
+        ((2, pieces, rp, h), BF16), ((2, pieces, rp, h), BF16),
+        ((2, pieces, rp, h), BF16), ((2, pieces, rp, h), BF16),
+        ((pieces, rp, h), F32), ((pieces, rp, h), F32),
+        ((F, n, w), BF16), ((n, w), BF16), ((F, n, w), BF16), ((F, n, w), F32),
     ]
     moved = pl.pallas_call(
         functools.partial(square_kernel, sizes),
@@ -931,10 +1057,10 @@
         out_specs=(vmem,) * len(shared),
         scratch_shapes=[pltpu.VMEM(shape, kind) for shape, kind in arrays] + [
             sem((7,)),
-            sem((2, 3, pieces)), sem((2, F, pieces)), sem((2, F, pieces)),
-            sem((3, pieces)), sem((F, pieces)), sem((3, parts)), sem((parts, F)),
-            sem((2, parts)), sem((2, parts)), sem((parts,)), sem((parts,)),
-            sem((1,)), sem((2, pieces)), sem((4, pieces)), sem((T, pieces)), sem((2, pieces)),
+            sem((2, 2 * T, pieces)), sem((2, F, pieces)), sem((2, F, pieces)),
+            sem((3, steps)), sem((F, steps)), sem((2, pieces)), sem((F, pieces)),
+            sem((2, pieces)), sem((2, pieces)), sem((2, pieces)), sem((2, pieces)),
+            sem((pieces,)), sem((F, pieces)), sem((F, pieces)), sem((3, pieces)), sem((pieces,)),
             sem((others, steps)), sem((others, steps)),
             sem((others, parts, tiles)), sem((others, parts, tiles)),
         ],

time: 89 us -> 84 us (0.944)
  Pallas kernels: 88.2 us -> 82.6 us
    pallas_call x1, Pallas kernels: 86 us -> 80.3 us  [square_body(): pl.pallas_call(functools.partial(square_kernel, sizes), out_shape=tuple((...]
where the time goes in v2:
time: 84 us; the launch traced here: 83.2 us
  Pallas kernels  82.6 us (98%)
    pallas_call x1, Pallas kernels, square_body(): pl.pallas_call(functools.partial(square_kernel, sizes), out_shape=tuple((...  80.3 us
    pallas_call x1, Pallas kernels, square_body(): pl.pallas_call(finish_kernel, out_shape=(jax.ShapeDtypeStruct((n, d), BF1...  2.21 us

profile of v2, /device:TPU:5, one launch (start us, length us, event | category | flops | bytes accessed | tf_op | source)
XLA Modules:
  0.0 83.2 jit_solution(8473544977969977999)
XLA Ops:
  0.6 80.3 %shard_map.94 = (bf16[4,256,512]{2,1,0:T(8,128)(2,1)S(1)}, bf16[1,4,256,512]{3,2,1,0:T(8,128)(2,1)S(1)}, bf16[2,2,256,512]{3,2,1,0:T(8,128)(2,1)S(1)}, bf16[1,2,...) custom-call(bf16[256,512]{1,0:T(8,128)(2,1)} %acts.1, bf16[256,512]{1,0:T(8,128)(2,1)} %cotangent.1, ...), custom_call_target="tpu_custom_call" | custom-call | tf_op jit(solution)/shard_map/pallas_call | solution.py:1053
  81.0 2.2 %shard_map.95 = (bf16[256,512]{1,0:T(8,128)(2,1)}, f32[512,1024]{1,0:T(8,128)}, f32[1024,512]{1,0:T(8,128)}) custom-call(bf16[4,256,512]{2,1,0:T(8,128)(2,1)S(1)} %get-tuple-element.8.gd_out, bf16[1,4,256,512]{3,2,1,0:T(8,128)(2,1)S(1)} %get-tuple-element.9.gd_in, bf16[2,2,256,512]{3,2,1,0:T(8,128)(2,1)S(1)} %get-tuple-element.10.gu_out, ...), custom_call_target="tpu_custom_call" | custom-call | tf_op jit(solution)/shard_map/pallas_call | solution.py:1078

commit v3 on v2

--- a/solution.py
+++ b/solution.py
@@ -450,7 +450,7 @@
     gd_out, gd_in, gu_out, gu_in, gi_in,
     acts_v, cot_v, pre_v, up_f32, up_scale_v, down_f32, down_scale_v,
     own, scaled_cols, acts_cols, pos_group, dpre_group, down_bf, up_bf,
-    pair_out, pair_in, far_out, far_in, own_f32, across_f32, gi_out, gi_mid, near_in, hub_f32,
+    pair_out, pair_in, far_out, far_in, sums, gi_out, gi_mid, near_in, hub_f32,
     load_sem,
     org_send, fwd_send, col_recv, act_send, act_recv, dpre_send, dpre_recv,
     pair_send, pair_recv, far_send, far_recv,
@@ -463,8 +463,8 @@
     w = down_store.shape[1]
     steps, gd_rows = gd_out.shape[0], gd_out.shape[1]
     parts, tiles, gu_rows, hp = gu_out.shape
-    pieces = col_recv.shape[2]
-    rp = n // pieces
+    pieces, strips = sums.shape[1], col_recv.shape[2]
+    rp, sp = n // pieces, n // strips
     norm_factor = 1.0 / math.sqrt(n * F * reps)
     r, f, z = lax.axis_index("rep"), lax.axis_index("fs"), lax.axis_index("tp")
     core, place = lax.rem(f, 2), lax.div(f, 2)
@@ -509,6 +509,12 @@
     def piece(at, p):
         return pl.ds(pl.multiple_of(at * n + p * rp, rp), rp)
 
+    def strip(at, p):
+        return pl.ds(pl.multiple_of(at * n + p * sp, sp), sp)
+
+    def strips_of(p):
+        return range(p * strips // pieces, (p + 1) * strips // pieces)
+
     def remote(src, dst, send, recv, where):
         return pltpu.make_async_remote_copy(
             src_ref=src, dst_ref=dst, send_sem=send, recv_sem=recv,
@@ -530,16 +536,16 @@
     falls = (z < f) & (z > 0)
 
     def originate(a, k, p, where):
-        at = pl.ds(p * rp, rp)
+        at = pl.ds(p * sp, sp)
         remote(
-            sources[a].at[at], cols[a].at[piece(f, p)],
+            sources[a].at[at], cols[a].at[strip(f, p)],
             org_send.at[a, k, p], col_recv.at[a, f, p], where,
         ).start()
 
     def originate_line(a):
         @pl.when(same)
         def _():
-            for p in range(pieces):
+            for p in range(strips):
                 @pl.when(z < T - 1)
                 def _():
                     originate(a, 1, p, {"fs": z, "tp": z + 1})
@@ -556,18 +562,30 @@
             def _():
                 cols[a][rows(f), :] = sources[a][...]
 
-    def spread_line(a):
+    def spread_inner(a):
         @pl.when(same)
         def _():
-            for p in range(pieces):
-                for k in range(1, T):
-                    @pl.when(z + k < T)
+            for p in range(strips):
+                for k in range(1, T - 1):
+                    @pl.when(z + k < T - 1)
                     def _():
                         originate(a, T + k, p, {"fs": z, "tp": z + k})
 
-                    @pl.when(z - k >= 0)
+                    @pl.when(z - k > 0)
                     def _():
                         originate(a, 1 + k, p, {"fs": z, "tp": z - k})
+
+    def spread_outer(a):
+        @pl.when(same)
+        def _():
+            for p in range(strips):
+                @pl.when(z == T - 2)
+                def _():
+                    originate(a, T + 1, p, {"fs": z, "tp": z + 1})
+
+                @pl.when(z == 1)
+                def _():
+                    originate(a, 2, p, {"fs": z, "tp": z - 1})
 
                 @pl.when(z != f)
                 def _():
@@ -580,12 +598,13 @@
     def originate_cross(a):
         @pl.when(jnp.logical_not(same))
         def _():
-            for p in range(pieces):
+            for p in range(strips):
                 originate(a, 1, p, {"fs": z, "tp": z_far})
-                originate(a, 0, p, {"fs": z})
+                if a == 0:
+                    originate(a, 0, p, {"fs": z})
 
     def pass_on(a, source, p, to):
-        ref = cols[a].at[piece(source, p)]
+        ref = cols[a].at[strip(source, p)]
         landed(ref, col_recv.at[a, source, p])
         remote(ref, ref, fwd_send.at[a, source, p], col_recv.at[a, source, p], {"tp": to}).start()
 
@@ -606,23 +625,38 @@
 
     def cross_rest(a, p):
         for source in (across, corner):
-            landed(cols[a].at[piece(source, p)], col_recv.at[a, source, p])
+            landed(cols[a].at[strip(source, p)], col_recv.at[a, source, p])
+
+    last_up, last_down = (z > f) & (z == T - 2), (z < f) & (z == 1)
+
+    def tip_forward(a, p):
+        @pl.when(last_up)
+        def _():
+            for source in (f, partner):
+                pass_on(a, source, p, z + 1)
+
+        @pl.when(last_down)
+        def _():
+            for source in (f, partner):
+                pass_on(a, source, p, z - 1)
 
     def line_landed(a, p):
-        @pl.when(z != f)
-        def _():
-            landed(cols[a].at[piece(f, p)], col_recv.at[a, f, p])
-
-        landed(cols[a].at[piece(partner, p)], col_recv.at[a, partner, p])
+        @pl.when(jnp.logical_not(last_up | last_down) & (z != f))
+        def _():
+            landed(cols[a].at[strip(f, p)], col_recv.at[a, f, p])
+
+        @pl.when(jnp.logical_not(last_up | last_down))
+        def _():
+            landed(cols[a].at[strip(partner, p)], col_recv.at[a, partner, p])
 
     def line_rest(a, p):
         @pl.when(jnp.logical_not(rises | falls) & (z != f))
         def _():
-            landed(cols[a].at[piece(f, p)], col_recv.at[a, f, p])
+            landed(cols[a].at[strip(f, p)], col_recv.at[a, f, p])
 
         @pl.when(jnp.logical_not(rises | falls))
         def _():
-            landed(cols[a].at[piece(partner, p)], col_recv.at[a, partner, p])
+            landed(cols[a].at[strip(partner, p)], col_recv.at[a, partner, p])
 
     def act_cols(c):
         return pl.ds(pl.multiple_of(c * gd_rows, gd_rows), gd_rows)
@@ -647,24 +681,21 @@
     originate_line(0)
     loads[2].wait()
     pos_group[rows(f), :] = jnp.maximum(pre_v[...].astype(F32), 0.0).astype(BF16)
-    early = (steps + 1) // 2
-    for c in range(early):
+    for c in range(steps):
         act_send_to(f, c, 0, {"fs": across})
+
+    loads[4].wait()
 
     @pl.when(jnp.logical_not(same))
     def _():
-        for c in range(early, steps):
-            act_send_to(f, c, 0, {"fs": across})
+        for p in range(strips):
+            originate(1, 0, p, {"fs": z})
         gi_in[2] = jnp.zeros((n, w), BF16)
 
     for c in range(steps):
         act_send_to(f, c, 1, {"fs": partner})
     loads[3].wait()
     down_bf[...] = down_f32[...].astype(BF16)
-
-    def late_act():
-        for c in range(early, steps):
-            act_send_to(f, c, 0, {"fs": across})
 
     def partial_of(target, p):
         return dot(scaled_cols[piece(target, p), :], down_bf[...], ((1,), (1,)))
@@ -676,51 +707,31 @@
             {"fs": partner},
         ).start()
 
-    def far_start(p):
-        value = partial_of(across, p)
-        landed(pair_in.at[0, p], pair_recv.at[0, p])
-        value = value + pair_in[0, p].astype(F32)
-        across_f32[p] = value
-        far_out[0, p] = value.astype(BF16)
+    def chip_sum(target, k, p):
+        value = partial_of(target, p)
+        landed(pair_in.at[k, p], pair_recv.at[k, p])
+        value = value + pair_in[k, p].astype(F32)
+        sums[k, p] = value
+        for e in range(parts):
+            far_out[k, e, p] = value[:, e * hp:(e + 1) * hp].astype(BF16)
+
+    def far_start(k, e, p):
         remote(
-            far_out.at[0, p], far_in.at[0, p], far_send.at[0, p], far_recv.at[0, p],
+            far_out.at[k, e, p], far_in.at[k, e, p], far_send.at[k, e, p], far_recv.at[k, e, p],
             {"fs": across},
         ).start()
 
     for p in range(pieces):
+        for t in strips_of(p):
+            @pl.when(direct)
+            def _():
+                cross_forward(0, t)
+
+            line_forward(0, t)
+
         @pl.when(direct)
         def _():
-            cross_forward(0, p)
-
-        line_forward(0, p)
-
-        @pl.when(direct)
-        def _():
             to_partner(corner, 0, p)
-
-    @pl.when(home)
-    def _():
-        late_act()
-
-    for p in range(pieces):
-        @pl.when(jnp.logical_not(direct))
-        def _():
-            cross_rest(0, p)
-            to_partner(corner, 0, p)
-
-        if p == 0:
-            @pl.when(same & jnp.logical_not(home))
-            def _():
-                late_act()
-
-        far_start(p)
-    loads[4].wait()
-    originate_cross(1)
-    for c in range(steps):
-        act_forward(c)
-    for p in range(pieces):
-        line_rest(0, p)
-    spread_line(1)
 
     def rep_copy(out, into, send, recv, at, p):
         to = lax.rem(r + p, reps)
@@ -740,39 +751,83 @@
             rep_copy(gd_out, gd_in, gd_send, gd_recv, (c,), p).start()
         return carry
 
-    lax.fori_loop(0, steps, down_step, 0)
+    def forward_and_down(c, carry):
+        act_forward(c)
+        return down_step(c, carry)
+
+    spread_inner(1)
+
+    @pl.when(direct)
+    def _():
+        for p in range(strips):
+            line_rest(0, p)
+        lax.fori_loop(0, steps, forward_and_down, 0)
+
+    half_steps = steps // 2
+    for p in range(pieces):
+        @pl.when(jnp.logical_not(direct))
+        def _():
+            for c in range(half_steps * p, steps if p == pieces - 1 else half_steps):
+                act_forward(c)
+            for t in strips_of(p):
+                cross_rest(0, t)
+            to_partner(corner, 0, p)
+
+        chip_sum(across, 0, p)
+        for e in range(parts):
+            far_start(0, e, p)
+    originate_cross(1)
+    spread_outer(1)
+
+    @pl.when(jnp.logical_not(direct))
+    def _():
+        for p in range(strips):
+            line_rest(0, p)
+        lax.fori_loop(0, steps, down_step, 0)
+
+
+    for p in range(strips):
+        tip_forward(1, p)
+
+    @pl.when(home)
+    def _():
+        for p in range(strips):
+            cross_forward(1, p)
+
     for p in range(pieces):
         to_partner(partner, 1, p)
     for p in range(pieces):
-        value = partial_of(f, p)
-        landed(pair_in.at[1, p], pair_recv.at[1, p])
-        value = value + pair_in[1, p].astype(F32)
-        own_f32[p] = value
-        far_out[1, p] = value.astype(BF16)
-        remote(
-            far_out.at[1, p], far_in.at[1, p], far_send.at[1, p], far_recv.at[1, p],
-            {"fs": across},
-        ).start()
+        chip_sum(f, 1, p)
+    for e in range(parts):
+        for p in range(pieces):
+            far_start(1, e, p)
     loads[5].wait()
     loads[6].wait()
     up_bf[...] = up_f32[...].astype(BF16)
 
-    def dpre_step(k, source, sums, p):
-        landed(far_in.at[k, p], far_recv.at[k, p])
-        value = sums[p] + far_in[k, p].astype(F32)
-        positive = pos_group[piece(source, p), :].astype(F32)
-        ref = dpre_group.at[piece(source, p)]
-        ref[...] = (2.0 * positive * value * up_scale_v[...]).astype(BF16)
-        remote(ref, ref, dpre_send.at[k, p], dpre_recv.at[source, p], {"fs": partner}).start()
+    def hidden(e):
+        return pl.ds(e * hp, hp)
+
+    def dpre_step(k, source, e, p):
+        landed(far_in.at[k, e, p], far_recv.at[k, e, p])
+        at = hidden(e)
+        value = sums[1 - k, p, :, at] + far_in[k, e, p].astype(F32)
+        positive = pos_group[piece(source, p), at].astype(F32)
+        ref = dpre_group.at[piece(source, p), at]
+        ref[...] = (2.0 * positive * value * up_scale_v[:, at]).astype(BF16)
+        remote(ref, ref, dpre_send.at[k, e, p], dpre_recv.at[e, source, p], {"fs": partner}).start()
+
+    def dpre_landed(source, e, p):
+        landed(dpre_group.at[piece(source, p), hidden(e)], dpre_recv.at[e, source, p])
+
+    @pl.when(hub)
+    def _():
+        for p in range(strips):
+            cross_forward(1, p)
 
     for p in range(pieces):
-        dpre_step(0, f, own_f32, p)
-
-        if p == 0:
-            @pl.when(hub)
-            def _():
-                for q in range(pieces):
-                    cross_forward(1, q)
+        for e in range(parts):
+            dpre_step(0, f, e, p)
 
     def half_rows(p):
         return pl.ds(p * rp, rp)
@@ -857,13 +912,9 @@
     for p in range(pieces):
         own_part(0, p)
     for p in range(pieces):
-        landed(dpre_group.at[piece(partner, p)], dpre_recv.at[partner, p])
+        for e in range(parts):
+            dpre_landed(partner, e, p)
         own_part(1, p)
-
-    @pl.when(home)
-    def _():
-        for p in range(pieces):
-            cross_forward(1, p)
 
     def up_step(e, q):
         value = dot(
@@ -874,29 +925,29 @@
         for p in range(1, reps):
             rep_copy(gu_out, gu_in, gu_send, gu_recv, (e, q), p).start()
 
-    for p in range(pieces):
-        dpre_step(1, across, across_f32, p)
-        landed(dpre_group.at[piece(corner, p)], dpre_recv.at[corner, p])
-        if p < pieces - 1:
-            cross_part(2, p)
-            cross_part(3, p)
-    for p in range(pieces):
-        @pl.when(jnp.logical_not(direct))
-        def _():
-            cross_rest(1, p)
-
-        line_landed(1, p)
     for e in range(parts):
+        last = e == parts - 1
+        for p in range(pieces):
+            dpre_step(1, across, e, p)
+            dpre_landed(corner, e, p)
+            if last:
+                cross_part(2, p)
+                cross_part(3, p)
+        if e == 0:
+            for p in range(strips):
+                @pl.when(jnp.logical_not(direct))
+                def _():
+                    cross_rest(1, p)
+
+                line_landed(1, p)
         for q in range(tiles):
             up_step(e, q)
-    cross_part(2, pieces - 1)
-    cross_part(3, pieces - 1)
+    for p in range(pieces):
+        for k in range(2):
+            own_sum(k, p)
     for p in range(pieces):
         for k in range(2, 4):
             cross_sum(k, p)
-    for p in range(pieces):
-        for k in range(2):
-            own_sum(k, p)
 
     relays = lax.div(z_far, 2) != place
     for p in range(pieces):
@@ -922,44 +973,50 @@
         def _():
             landed(gi_in.at[2, half_rows(p)], gi_recv.at[2, p])
 
-    for p in range(pieces):
+    for p in range(strips):
         for a in range(2):
             @pl.when(same & (z != f) | jnp.logical_not(same))
             def _():
-                left_for(own.at[half_rows(p)], org_send.at[a, 0, p])
+                left_for(own.at[pl.ds(p * sp, sp)], org_send.at[a, 0, p])
 
             @pl.when(direct)
             def _():
                 for source in (across, corner):
-                    left_for(own.at[half_rows(p)], fwd_send.at[a, source, p])
+                    left_for(own.at[pl.ds(p * sp, sp)], fwd_send.at[a, source, p])
 
         @pl.when(jnp.logical_not(same))
         def _():
             for a in range(2):
-                left_for(own.at[half_rows(p)], org_send.at[a, 1, p])
+                left_for(own.at[pl.ds(p * sp, sp)], org_send.at[a, 1, p])
 
         @pl.when(same & (z < T - 1))
         def _():
-            left_for(own.at[half_rows(p)], org_send.at[0, 1, p])
+            left_for(own.at[pl.ds(p * sp, sp)], org_send.at[0, 1, p])
 
         @pl.when(same & (z > 0))
         def _():
-            left_for(own.at[half_rows(p)], org_send.at[0, 2, p])
+            left_for(own.at[pl.ds(p * sp, sp)], org_send.at[0, 2, p])
 
         @pl.when(rises | falls)
         def _():
             for source in (f, partner):
-                left_for(own.at[half_rows(p)], fwd_send.at[0, source, p])
-
-        for k in range(1, T):
-            @pl.when(same & (z + k < T))
-            def _():
-                left_for(own.at[half_rows(p)], org_send.at[1, T + k, p])
-
-            @pl.when(same & (z - k >= 0))
-            def _():
-                left_for(own.at[half_rows(p)], org_send.at[1, 1 + k, p])
-
+                left_for(own.at[pl.ds(p * sp, sp)], fwd_send.at[0, source, p])
+
+        for k in range(1, T - 1):
+            @pl.when(same & ((z + k < T - 1) | ((k == 1) & (z + k < T))))
+            def _():
+                left_for(own.at[pl.ds(p * sp, sp)], org_send.at[1, T + k, p])
+
+            @pl.when(same & ((z - k > 0) | ((k == 1) & (z - k >= 0))))
+            def _():
+                left_for(own.at[pl.ds(p * sp, sp)], org_send.at[1, 1 + k, p])
+
+        @pl.when(last_up | last_down)
+        def _():
+            for source in (f, partner):
+                left_for(own.at[pl.ds(p * sp, sp)], fwd_send.at[1, source, p])
+
+    for p in range(pieces):
         @pl.when(jnp.logical_not(home))
         def _():
             left_for(own.at[half_rows(p)], gi_send.at[0, p])
@@ -972,9 +1029,10 @@
             left_for(own.at[half_rows(p)], relay_send.at[p])
 
         for k in range(2):
-            left_for(dpre_group.at[piece(f, p)], dpre_send.at[k, p])
             left_for(pair_out.at[k, p], pair_send.at[k, p])
-            left_for(far_out.at[k, p], far_send.at[k, p])
+            for e in range(parts):
+                left_for(dpre_group.at[piece(f, p), hidden(e)], dpre_send.at[k, e, p])
+                left_for(far_out.at[k, e, p], far_send.at[k, e, p])
     for k in range(3):
         for c in range(steps):
             left_for(pos_group.at[rows(f), act_cols(c)], act_send.at[k, c])
@@ -1028,6 +1086,7 @@
     parts = 2 if h % 256 == 0 else 1
     pieces = 2 if n % 32 == 0 else 1
     tiles = 2 if w % 256 == 0 else 1
+    strips = 2 * pieces if n % 64 == 0 else pieces
     hp, rp = h // parts, n // pieces
     gd_rows = fitting(h, 256)
     steps = h // gd_rows
@@ -1046,8 +1105,8 @@
         ((F * n, h), BF16), ((F * n, h), BF16),
         ((h, w), BF16), ((w, h), BF16),
         ((2, pieces, rp, h), BF16), ((2, pieces, rp, h), BF16),
-        ((2, pieces, rp, h), BF16), ((2, pieces, rp, h), BF16),
-        ((pieces, rp, h), F32), ((pieces, rp, h), F32),
+        ((2, parts, pieces, rp, hp), BF16), ((2, parts, pieces, rp, hp), BF16),
+        ((2, pieces, rp, h), F32),
         ((F, n, w), BF16), ((n, w), BF16), ((F, n, w), BF16), ((F, n, w), F32),
     ]
     moved = pl.pallas_call(
@@ -1057,9 +1116,9 @@
         out_specs=(vmem,) * len(shared),
         scratch_shapes=[pltpu.VMEM(shape, kind) for shape, kind in arrays] + [
             sem((7,)),
-            sem((2, 2 * T, pieces)), sem((2, F, pieces)), sem((2, F, pieces)),
-            sem((3, steps)), sem((F, steps)), sem((2, pieces)), sem((F, pieces)),
-            sem((2, pieces)), sem((2, pieces)), sem((2, pieces)), sem((2, pieces)),
+            sem((2, 2 * T, strips)), sem((2, F, strips)), sem((2, F, strips)),
+            sem((3, steps)), sem((F, steps)), sem((2, parts, pieces)), sem((parts, F, pieces)),
+            sem((2, pieces)), sem((2, pieces)), sem((2, parts, pieces)), sem((2, parts, pieces)),
             sem((pieces,)), sem((F, pieces)), sem((F, pieces)), sem((3, pieces)), sem((pieces,)),
             sem((others, steps)), sem((others, steps)),
             sem((others, parts, tiles)), sem((others, parts, tiles)),

time: 84 us -> 79.4 us (0.945)
  Pallas kernels: 82.6 us -> 78.6 us
    pallas_call x1, Pallas kernels: 80.3 us -> 76.4 us  [square_body(): pl.pallas_call(functools.partial(square_kernel, sizes), out_shape=tuple((...]
where the time goes in v3:
time: 79.4 us; the launch traced here: 79.3 us
  Pallas kernels  78.6 us (99%)
    pallas_call x1, Pallas kernels, square_body(): pl.pallas_call(functools.partial(square_kernel, sizes), out_shape=tuple((...  76.4 us
    pallas_call x1, Pallas kernels, square_body(): pl.pallas_call(finish_kernel, out_shape=(jax.ShapeDtypeStruct((n, d), BF1...  2.21 us

profile of v3, /device:TPU:5, one launch (start us, length us, event | category | flops | bytes accessed | tf_op | source)
XLA Modules:
  0.0 79.3 jit_solution(9922393386527583332)
XLA Ops:
  0.6 76.4 %shard_map.94 = (bf16[4,256,512]{2,1,0:T(8,128)(2,1)S(1)}, bf16[1,4,256,512]{3,2,1,0:T(8,128)(2,1)S(1)}, bf16[2,2,256,512]{3,2,1,0:T(8,128)(2,1)S(1)}, bf16[1,2,...) custom-call(bf16[256,512]{1,0:T(8,128)(2,1)} %acts.1, bf16[256,512]{1,0:T(8,128)(2,1)} %cotangent.1, ...), custom_call_target="tpu_custom_call" | custom-call | tf_op jit(solution)/shard_map/pallas_call | solution.py:1112
  77.1 2.2 %shard_map.95 = (bf16[256,512]{1,0:T(8,128)(2,1)}, f32[512,1024]{1,0:T(8,128)}, f32[1024,512]{1,0:T(8,128)}) custom-call(bf16[4,256,512]{2,1,0:T(8,128)(2,1)S(1)} %get-tuple-element.8.gd_out, bf16[1,4,256,512]{3,2,1,0:T(8,128)(2,1)S(1)} %get-tuple-element.9.gd_in, bf16[2,2,256,512]{3,2,1,0:T(8,128)(2,1)S(1)} %get-tuple-element.10.gu_out, ...), custom_call_target="tpu_custom_call" | custom-call | tf_op jit(solution)/shard_map/pallas_call | solution.py:1137

commit v4 on v3

--- a/solution.py
+++ b/solution.py
@@ -695,10 +695,10 @@
     for c in range(steps):
         act_send_to(f, c, 1, {"fs": partner})
     loads[3].wait()
-    down_bf[...] = down_f32[...].astype(BF16)
+    down_bf[...] = down_f32[...].T.astype(BF16)
 
     def partial_of(target, p):
-        return dot(scaled_cols[piece(target, p), :], down_bf[...], ((1,), (1,)))
+        return dot(scaled_cols[piece(target, p), :], down_bf[...], ((1,), (0,)))
 
     def to_partner(target, k, p):
         pair_out[k, p] = partial_of(target, p).astype(BF16)
@@ -763,18 +763,17 @@
             line_rest(0, p)
         lax.fori_loop(0, steps, forward_and_down, 0)
 
-    half_steps = steps // 2
     for p in range(pieces):
         @pl.when(jnp.logical_not(direct))
         def _():
-            for c in range(half_steps * p, steps if p == pieces - 1 else half_steps):
+            for c in range(p * steps // pieces, (p + 1) * steps // pieces):
                 act_forward(c)
             for t in strips_of(p):
                 cross_rest(0, t)
             to_partner(corner, 0, p)
 
         chip_sum(across, 0, p)
-        for e in range(parts):
+        for e in range(parts if p == 0 else 1):
             far_start(0, e, p)
     originate_cross(1)
     spread_outer(1)
@@ -798,12 +797,16 @@
         to_partner(partner, 1, p)
     for p in range(pieces):
         chip_sum(f, 1, p)
-    for e in range(parts):
+    for p in range(pieces):
+        far_start(1, 0, p)
+    for e in range(1, parts):
+        for p in range(1, pieces):
+            far_start(0, e, p)
         for p in range(pieces):
             far_start(1, e, p)
     loads[5].wait()
     loads[6].wait()
-    up_bf[...] = up_f32[...].astype(BF16)
+    up_bf[...] = up_f32[...].T.astype(BF16)
 
     def hidden(e):
         return pl.ds(e * hp, hp)
@@ -826,7 +829,7 @@
             cross_forward(1, p)
 
     for p in range(pieces):
-        for e in range(parts):
+        for e in range(parts if p == 0 else 1):
             dpre_step(0, f, e, p)
 
     def half_rows(p):
@@ -834,7 +837,7 @@
 
     def input_part(k, p):
         target = (f, partner, across, corner)[k]
-        return dot(dpre_group[piece(target, p), :], up_bf[...], ((1,), (1,)))
+        return dot(dpre_group[piece(target, p), :], up_bf[...], ((1,), (0,)))
 
     def input_sum(k, p, value):
         landed(near_in.at[k, half_rows(p)], near_recv.at[k, p])
@@ -909,12 +912,13 @@
         def _():
             input_send(k, p, gi_mid, mid_recv, {"fs": target})
 
-    for p in range(pieces):
+    def own_parts(p):
         own_part(0, p)
-    for p in range(pieces):
-        for e in range(parts):
+        for e in range(parts) if p == 0 else range(parts - 1, parts):
             dpre_landed(partner, e, p)
         own_part(1, p)
+
+    own_parts(0)
 
     def up_step(e, q):
         value = dot(
@@ -927,11 +931,20 @@
 
     for e in range(parts):
         last = e == parts - 1
+        if last:
+            for p in range(1, pieces):
+                if e > 0:
+                    dpre_step(0, f, e, p)
+                own_parts(p)
+        else:
+            for p in range(1, pieces):
+                dpre_landed(partner, e, p)
         for p in range(pieces):
             dpre_step(1, across, e, p)
+            if last:
+                cross_part(2, p)
             dpre_landed(corner, e, p)
             if last:
-                cross_part(2, p)
                 cross_part(3, p)
         if e == 0:
             for p in range(strips):
@@ -1103,7 +1116,7 @@
         ((w, h), F32), ((1, h), F32), ((h, w), F32), ((1, d * T), F32),
         ((n, d), BF16), ((F * n, w), BF16), ((F * n, w), BF16),
         ((F * n, h), BF16), ((F * n, h), BF16),
-        ((h, w), BF16), ((w, h), BF16),
+        ((w, h), BF16), ((h, w), BF16),
         ((2, pieces, rp, h), BF16), ((2, pieces, rp, h), BF16),
         ((2, parts, pieces, rp, hp), BF16), ((2, parts, pieces, rp, hp), BF16),
         ((2, pieces, rp, h), F32),

time: 79.4 us -> 77.9 us (0.981)
  Pallas kernels: 78.6 us -> 77 us
    pallas_call x1, Pallas kernels: 76.4 us -> 74.8 us  [square_body(): pl.pallas_call(functools.partial(square_kernel, sizes), out_shape=tuple((...]
where the time goes in v4:
time: 77.9 us; the launch traced here: 77.6 us
  Pallas kernels  77 us (99%)
    pallas_call x1, Pallas kernels, square_body(): pl.pallas_call(functools.partial(square_kernel, sizes), out_shape=tuple((...  74.8 us
    pallas_call x1, Pallas kernels, square_body(): pl.pallas_call(finish_kernel, out_shape=(jax.ShapeDtypeStruct((n, d), BF1...  2.21 us

profile of v4, /device:TPU:5, one launch (start us, length us, event | category | flops | bytes accessed | tf_op | source)
XLA Modules:
  0.0 77.6 jit_solution(736166888252885353)
XLA Ops:
  0.6 74.8 %shard_map.94 = (bf16[4,256,512]{2,1,0:T(8,128)(2,1)S(1)}, bf16[1,4,256,512]{3,2,1,0:T(8,128)(2,1)S(1)}, bf16[2,2,256,512]{3,2,1,0:T(8,128)(2,1)S(1)}, bf16[1,2,...) custom-call(bf16[256,512]{1,0:T(8,128)(2,1)} %acts.1, bf16[256,512]{1,0:T(8,128)(2,1)} %cotangent.1, ...), custom_call_target="tpu_custom_call" | custom-call | tf_op jit(solution)/shard_map/pallas_call | solution.py:1125
  75.4 2.2 %shard_map.95 = (bf16[256,512]{1,0:T(8,128)(2,1)}, f32[512,1024]{1,0:T(8,128)}, f32[1024,512]{1,0:T(8,128)}) custom-call(bf16[4,256,512]{2,1,0:T(8,128)(2,1)S(1)} %get-tuple-element.8.gd_out, bf16[1,4,256,512]{3,2,1,0:T(8,128)(2,1)S(1)} %get-tuple-element.9.gd_in, bf16[2,2,256,512]{3,2,1,0:T(8,128)(2,1)S(1)} %get-tuple-element.10.gu_out, ...), custom_call_target="tpu_custom_call" | custom-call | tf_op jit(solution)/shard_map/pallas_call | solution.py:1150
